TPU v7x, 512 devices: a whole 4x8x8 slice. The times are simulated.
512 devices in a mesh: sp: 64 (over z, y), tp: 8 (over x, core).
Axes of the slice: x: 4, y: 8, z: 8, core: 2. Of those that a mesh axis runs over, the one named last changes fastest.
Arguments:
- queries: bfloat16 [16384, 1024], P('sp', 'tp'), may hold values from -6 to 6
- keys: bfloat16 [16384, 256], P('sp'), may hold values from -6 to 6
- values: bfloat16 [16384, 256], P('sp'), may hold values from -6 to 6
- query_gain: float32 [128], replicated, may hold values from 1.4 to 5.5
- key_gain: float32 [128], replicated, may hold values from 1.4 to 5.5
- residual_in: bfloat16 [16384, 2048], P(('sp', 'tp')), may hold values from -6 to 6
- out_weight: bfloat16 [1024, 2048], P('tp'), may hold values from -0.1875 to 0.1875
- norm_gain: float32 [2048], replicated, may hold values from 0.1 to 1.9
- gate_weight: bfloat16 [2048, 3072], P('sp', 'tp'), may hold values from -0.125 to 0.125
- up_weight: bfloat16 [2048, 3072], P('sp', 'tp'), may hold values from -0.125 to 0.125
- down_weight: bfloat16 [3072, 2048], P('tp', 'sp'), may hold values from -0.109375 to 0.109375
Outputs:
- result: bfloat16 [16384, 2048], P(('sp', 'tp'))
All inputs are finite; a program needn't handle non-finite values.
Results may differ from a plain program's by a relative error of at most 0.017.
Values may be sent and summed in bfloat16 or wider, within the bound.
A program may use at most 64 MiB of HBM per device.

v0:
```python
import math

import jax
import jax.numpy as jnp
from jax import lax
from jax.sharding import Mesh
from jax.sharding import PartitionSpec as P

Q_HEADS = 8
KV_HEADS = 2
GRID_WIDTH = 64
SP = ("sp_0", "sp_1")
SP_TP = ("sp_0", "sp_1", "tp")


EPS = 1e-06
ROPE_BASE = 10000.0


def side_by_side(arrays, axis, dim, along):
    widths = [a.shape[along] for a in arrays]
    both = jnp.concatenate(arrays, axis=along)
    result = lax.all_gather(both, axis, axis=dim, tiled=True)
    return tuple(jnp.split(result, [sum(widths[:k]) for k in range(1, len(widths))], axis=along))


def in_order(parts, dim):
    parts = jnp.moveaxis(parts, 0, dim)
    dims = parts.shape
    return parts.reshape(*dims[:dim], dims[dim] * dims[dim + 1], *dims[dim + 2 :])


def stacked_from(value, axes, turns):
    parts = value[None]
    for k in turns:
        parts = lax.all_gather(parts, axes[k], axis=0, tiled=True)
    block = [lax.axis_size(axes[k]) for k in reversed(turns)]
    parts = parts.reshape(*block, *value.shape)
    turned = sorted(range(len(turns)), key=lambda place: turns[len(turns) - 1 - place])
    return parts.transpose(*turned, *range(len(turns), parts.ndim)).reshape(-1, *value.shape)


def whole_of(value, axes, turns, dim):
    return in_order(stacked_from(value, axes, turns), dim)


def split_up(value, dim, size):
    before, after = (value.shape[:dim], value.shape[dim + 1 :])
    return jnp.moveaxis(value.reshape(*before, size, -1, *after), dim, 0)


def sent_and_summed(value, axis, dim):
    parts = split_up(value, dim, lax.axis_size(axis))
    arrived = lax.all_to_all(parts, axis, split_axis=0, concat_axis=0, tiled=True)
    return arrived.astype(jnp.float32).sum(axis=0)


def sent_to_all(value, axis):
    size = lax.axis_size(axis)
    return lax.all_to_all(
        jnp.broadcast_to(value[None], (size, *value.shape)), axis, 0, 0, tiled=True
    )


def gather_directly(value, axis, dim):
    return in_order(sent_to_all(value, axis), dim)


def normalize(wide_values, gain):
    wide = wide_values.astype(jnp.float32)
    return wide * lax.rsqrt(jnp.mean(wide * wide, axis=-1, keepdims=True) + EPS) * gain


def rotate_pair(segment, angles):
    half_size = segment.shape[-1] // 2
    first = segment[..., :half_size]
    second = segment[..., half_size:]
    cosine = jnp.cos(angles)[:, None, :]
    sine_part = jnp.sin(angles)[:, None, :]
    return jnp.concatenate(
        [first * cosine - second * sine_part, second * cosine + first * sine_part], axis=-1
    )


def grid_rotary(head_rows, positions):
    head_size = head_rows.shape[-1]
    half_size = head_size // 2
    quarter = head_size // 4
    inverse = ROPE_BASE ** (-jnp.arange(quarter, dtype=jnp.float32) * 2.0 / half_size)
    row_angles = (positions // GRID_WIDTH).astype(jnp.float32)[:, None] * inverse
    col_angles = (positions % GRID_WIDTH).astype(jnp.float32)[:, None] * inverse
    return jnp.concatenate(
        [
            rotate_pair(head_rows[..., :half_size], row_angles),
            rotate_pair(head_rows[..., half_size:], col_angles),
        ],
        axis=-1,
    )


def gated(gate_part, lifted):
    return (jax.nn.silu(gate_part) * lifted).astype(jnp.bfloat16)


def local(
    queries,
    keys,
    values,
    query_gain,
    key_gain,
    residual_in,
    out_weight,
    norm_gain,
    gate_weight,
    up_weight,
    down_weight,
):
    tok_rows = queries.shape[0]
    head_size = query_gain.shape[0]
    local_heads = queries.shape[1] // head_size
    tp_index = lax.axis_index("tp")
    gate_full, up_full = side_by_side((gate_weight, up_weight), SP, 0, 1)
    down_full = whole_of(down_weight, SP, (0, 1), 1)
    positions = lax.axis_index(SP) * tok_rows + jnp.arange(tok_rows, dtype=jnp.int32)
    key_head = tp_index * local_heads // (Q_HEADS // KV_HEADS)
    own_keys = lax.dynamic_slice_in_dim(keys, key_head * head_size, head_size, 1)
    own_values = lax.dynamic_slice_in_dim(values, key_head * head_size, head_size, 1)
    turned_keys = grid_rotary(
        normalize(own_keys.reshape(tok_rows, 1, head_size), key_gain), positions
    )
    turned_keys = turned_keys.reshape(tok_rows, head_size).astype(jnp.bfloat16)
    turned_queries = grid_rotary(
        normalize(queries.reshape(tok_rows, local_heads, head_size), query_gain), positions
    )
    turned_queries = turned_queries.reshape(tok_rows * local_heads, head_size).astype(jnp.bfloat16)
    score_scale = head_size ** (-0.5)

    def attend_block(running, block_pair):
        peak_score, weight_total, weighted = running
        block_keys, block_values = block_pair
        scores = (
            lax.dot_general(
                turned_queries,
                block_keys,
                (((1,), (1,)), ((), ())),
                preferred_element_type=jnp.float32,
            )
            * score_scale
        )
        new_peak = jnp.maximum(peak_score, jnp.max(scores, axis=1))
        factor = jnp.exp(peak_score - new_peak)
        raw = jnp.exp(scores - new_peak[:, None])
        weight_total = weight_total * factor + jnp.sum(raw, axis=1)
        weighted = weighted * factor[:, None] + jnp.dot(
            raw.astype(jnp.bfloat16), block_values, preferred_element_type=jnp.float32
        )
        return ((new_peak, weight_total, weighted), None)

    row_count = tok_rows * local_heads
    start_carry = (
        jnp.full((row_count,), -1e30, jnp.float32),
        jnp.zeros((row_count,), jnp.float32),
        jnp.zeros((row_count, head_size), jnp.float32),
    )
    piece_keys, piece_values = side_by_side((turned_keys, own_values), SP, 0, 1)
    span = math.gcd(piece_keys.shape[0], 512)
    blocks = piece_keys.shape[0] // span
    stacked = (
        piece_keys.reshape(blocks, span, head_size),
        piece_values.reshape(blocks, span, head_size),
    )
    updated, unused = lax.scan(attend_block, start_carry, stacked)
    peak_score, weight_total, weighted = updated
    attended = (weighted / weight_total[:, None]).astype(jnp.bfloat16)
    attention_out = sent_and_summed(
        jnp.dot(attended, out_weight, preferred_element_type=jnp.float32).astype(jnp.bfloat16),
        "tp",
        0,
    )
    middle = (residual_in.astype(jnp.float32) + attention_out).astype(jnp.bfloat16)
    normed = gather_directly(normalize(middle, norm_gain).astype(jnp.bfloat16), "tp", 0)
    hidden = gated(
        jnp.dot(normed, gate_full, preferred_element_type=jnp.float32),
        jnp.dot(normed, up_full, preferred_element_type=jnp.float32),
    )
    partials = jnp.dot(hidden, down_full, preferred_element_type=jnp.float32)
    mixer_out = sent_and_summed(partials.astype(jnp.bfloat16), "tp", 0)
    return (middle.astype(jnp.float32) + mixer_out).astype(jnp.bfloat16)


def solution(mesh):
    finer = Mesh(mesh.devices.reshape(8, 8, mesh.shape["tp"]), ("sp_0", "sp_1", "tp"))
    in_specs = (
        P(SP, "tp"),
        P(SP, None),
        P(SP, None),
        P(),
        P(),
        P(SP_TP, None),
        P("tp", None),
        P(),
        P(SP, "tp"),
        P(SP, "tp"),
        P("tp", SP),
    )
    out_specs = P(SP_TP, None)
    return jax.shard_map(local, mesh=finer, in_specs=in_specs, out_specs=out_specs, check_vma=False)
```

profile of v0, /device:TPU:1, one launch (start us, length us, event | category | flops | bytes accessed | tf_op | source)
XLA Modules:
  0.0 299.4 jit_solution(13438292741110055341)
XLA Ops:
  11.4 26.1 %all-gather = bf16[3072,32]{0,1:T(8,128)(2,1)S(1)} all-gather(bf16[384,32]{0,1:T(8,128)(2,1)} %param.23), channel_id=2, replica_groups=mesh['sp_0'=8,'sp_1'=8,'tp'=8] {'sp_0'}, dimensions={0}, use_global_device_ids=true | all-gather | bytes 221184 | tf_op jit(solution)/shard_map/all_gather | solution.py:36
  38.2 1.4 pad_maximum_fusion.1
  39.8 80.1 %all-gather.5.cloned.1.call-done = bf16[16384,256]{0,1:T(8,128)(2,1)} async-done(((bf16[256,256]{0,1:T(8,128)(2,1)}), bf16[16384,256]{0,1:T(8,128)(2,1)}) %all-gather.5.cloned.1.call-update) | async-done | bytes 8388624 | tf_op jit(solution)/shard_map/all_gather | solution.py:23
  119.9 5.8 %fusion.78 = (bf16[16384,128]{0,1:T(8,128)(2,1)}, bf16[16384,128]{0,1:T(8,128)(2,1)}) fusion(bf16[16384,256]{0,1:T(8,128)(2,1)} %all-gather.5.cloned.1.call-done), kind=kLoop, calls=%fused_computation.112 | loop fusion | bytes 16777216 | tf_op jit(solution)/shard_map/split | solution.py:24
  125.7 6.4 %copy.23 = bf16[16384,128]{1,0:T(8,128)(2,1)} copy(bf16[16384,128]{0,1:T(8,128)(2,1)} %get-tuple-element.97) | data formatting | bytes 8388608
  132.0 6.4 %copy.24 = bf16[16384,128]{1,0:T(8,128)(2,1)} copy(bf16[16384,128]{0,1:T(8,128)(2,1)} %get-tuple-element.96) | data formatting | bytes 8388608
  138.4 81.8 %while.15 = (s32[]{:T(128)}, f32[256]{0:T(256)S(1)}, f32[256]{0:T(256)S(1)}, f32[256,128]{1,0:T(8,128)S(1)}, bf16[32,512,128]{2,1,0:T(8,128)(2,1)}, /*index=5*/b...) while((s32[]{:T(128)}, f32[256]{0:T(256)S(1)}, ...), condition=%wide.region_5.6_spmd.clone, body=%wide.region_2.5_spmd.clone.sunk | while | flops 67994880 | bytes 2180201 | solution.py:172
  139.8 1.2 convolution_add_fusion.2
  142.3 1.2 convolution_add_fusion.2
  143.5 1.2 fusion.94
  144.9 1.2 convolution_add_fusion.2
  147.4 1.2 convolution_add_fusion.2
  148.7 1.2 fusion.94
  150.0 1.2 convolution_add_fusion.2
  151.2 1.2 fusion.94
  152.5 1.2 convolution_add_fusion.2
  153.8 1.2 fusion.94
  155.1 1.2 convolution_add_fusion.2
  156.3 1.2 fusion.94
  157.7 1.2 convolution_add_fusion.2
  160.2 1.2 convolution_add_fusion.2
  161.4 1.2 fusion.94
  162.8 1.2 convolution_add_fusion.2
  165.3 1.2 convolution_add_fusion.2
  166.6 1.2 fusion.94
  167.9 1.2 convolution_add_fusion.2
  170.4 1.2 convolution_add_fusion.2
  171.7 1.2 fusion.94
  173.0 1.2 convolution_add_fusion.2
  175.6 1.2 convolution_add_fusion.2
  176.8 1.2 fusion.94
  178.1 1.2 convolution_add_fusion.2
  180.7 1.2 convolution_add_fusion.2
  183.2 1.2 convolution_add_fusion.2
  184.4 1.2 fusion.94
  185.8 1.2 convolution_add_fusion.2
  188.3 1.2 convolution_add_fusion.2
  189.5 1.2 fusion.94
  190.9 1.2 convolution_add_fusion.2
  193.4 1.2 convolution_add_fusion.2
  194.7 1.2 fusion.94
  196.0 1.2 convolution_add_fusion.2
  197.2 1.2 fusion.94
  198.6 1.2 convolution_add_fusion.2
  201.1 1.2 convolution_add_fusion.2
  202.3 1.2 fusion.94
  203.7 1.2 convolution_add_fusion.2
  204.9 1.2 fusion.94
  206.2 1.2 convolution_add_fusion.2
  207.4 1.2 fusion.94
  208.8 1.2 convolution_add_fusion.2
  211.3 1.2 convolution_add_fusion.2
  212.6 1.2 fusion.94
  213.9 1.2 convolution_add_fusion.2
  216.4 1.2 convolution_add_fusion.2
  217.7 1.2 fusion.94
  219.0 1.2 convolution_add_fusion.2
  220.7 24.3 %all_to_all.15 = bf16[8,32,2048]{2,1,0:T(8,128)(2,1)S(1)} all-to-all(bf16[8,32,2048]{2,1,0:T(8,128)(2,1)S(1)} %bitcast.46), channel_id=1, replica_groups=mesh['sp_0'=8,'sp_1'=8,'tp'=8] {'tp'}, dimensions={0} | all-to-all | bytes 2097152 | tf_op jit(solution)/shard_map/all_to_all | solution.py:54
  246.6 4.5 %all-to-all-start.1 = ((bf16[8,32,2048]{2,1,0:T(8,128)(2,1)}), bf16[8,32,2048]{2,1,0:T(8,128)(2,1)S(1)}, u32[]{:S(2)}, u32[]{:S(2)}) async-start(bf16[8,32,2048]{2,1,0:T(8,128)(2,1)} %broadcast_in_dim.13), calls=%async_computation.1 | async-start | bytes 2097152 | tf_op jit(solution)/shard_map/all_to_all | solution.py:60
  251.1 2.3 copy.22
  253.4 12.6 %all-to-all-done.1 = bf16[8,32,2048]{2,1,0:T(8,128)(2,1)S(1)} async-done(((bf16[8,32,2048]{2,1,0:T(8,128)(2,1)}), bf16[8,32,2048]{2,1,0:T(8,128)(2,1)S(1)}, u32[]{:S(2)}, u32[]{:S(2)}) %all-to-all-start.1) | async-done | bytes 1048608 | tf_op jit(solution)/shard_map/all_to_all | solution.py:60
  266.1 2.9 fusion.14
  268.9 3.8 %convolution_convert_fusion = bf16[256,2048]{1,0:T(8,128)(2,1)} fusion(bf16[384,2048]{0,1:T(8,128)(2,1)S(1)} %bitcast.48, bf16[256,2048]{1,0:T(8,128)(2,1)S(1)} %bitcast.50, bf16[2048,768]{1,0:T(8,128)(2,1)} %all-gather.7.cloned.1.call-done, f32[256,384]{1,0:T(8,128)} %fusion.14), kind=kOutput, calls=%fused_computation.18 | convolution fusion | flops 806420480 | bytes 5636096 | tf_op jit(solution)/shard_map/dot_general | solution.py:186
  272.7 19.4 %all_to_all.16 = bf16[8,32,2048]{2,1,0:T(8,128)(2,1)S(1)} all-to-all(bf16[8,32,2048]{2,1,0:T(8,128)(2,1)} %bitcast.51), channel_id=1, replica_groups=mesh['sp_0'=8,'sp_1'=8,'tp'=8] {'tp'}, dimensions={0} | all-to-all | bytes 2097152 | tf_op jit(solution)/shard_map/all_to_all | solution.py:54
  (185 shorter events, 29.6 us)
Async XLA Ops:
  6.5 213.7 %copy-start = (bf16[128,2048]{1,0:T(8,128)(2,1)S(1)}, bf16[128,2048]{1,0:T(8,128)(2,1)}, u32[]{:S(2)}) copy-start(bf16[128,2048]{1,0:T(8,128)(2,1)} %param.19) | copy-start | bytes 1572868
  6.5 113.3 %all-gather.5.cloned.1.call-start = ((), (), s32[]{:S(2)}) async-start(), calls=%async_computation.3 | async-start | bytes 8519680 | tf_op jit(solution)/shard_map/all_gather | solution.py:23
  11.3 239.7 %all-gather.9.cloned.1.call-start = ((), (), s32[]{:S(2)}) async-start(), calls=%async_computation.5 | async-start | bytes 1769472 | tf_op jit(solution)/shard_map/all_gather | solution.py:36
  38.2 215.2 %all-gather.7.cloned.1.call-start = ((), (), s32[]{:S(2)}) async-start(), calls=%async_computation.4 | async-start | bytes 3194880 | tf_op jit(solution)/shard_map/all_gather | solution.py:23
  220.2 25.0 %copy-start.1 = (bf16[32,2048]{1,0:T(8,128)(2,1)S(1)}, bf16[32,2048]{1,0:T(8,128)(2,1)}, u32[]{:S(2)}) copy-start(bf16[32,2048]{1,0:T(8,128)(2,1)} %param.18) | copy-start | bytes 393220
  220.2 25.1 %copy-start.2 = (f32[2048]{0:T(1024)S(1)}, f32[2048]{0:T(1024)}, u32[]{:S(2)}) copy-start(f32[2048]{0:T(1024)} %param.20) | copy-start | bytes 24580
  246.6 19.5 %all-to-all-start.1 = ((bf16[8,32,2048]{2,1,0:T(8,128)(2,1)}), bf16[8,32,2048]{2,1,0:T(8,128)(2,1)S(1)}, u32[]{:S(2)}, u32[]{:S(2)}) async-start(bf16[8,32,2048]{2,1,0:T(8,128)(2,1)} %broadcast_in_dim.13), calls=%async_computation.1 | async-start | bytes 2097152 | tf_op jit(solution)/shard_map/all_to_all | solution.py:60
Sparse Core Ops, SparseCore 0:
  11.5 108.3 all-gather.4
  122.0 38.1 all-gather.8
  163.1 85.2 all-gather.6
where the time goes:
time: 301 us; the launch traced here: 299 us
  waiting for transfers between devices  92.8 us (31%)
  matrix products  82.6 us (27%)
  blocking collectives  69.7 us (23%)
  local copies, waits for them, and re-layouts  25 us (8%)
  between operations  13.3 us (4%)
  other arithmetic  9.95 us (3%)
  starting transfers between devices  4.58 us (2%)
    all_gather x2, waiting for transfers between devices, side_by_side(): result = lax.all_gather(both, axis, axis=dim, tiled=True)  80.1 us
    all_to_all x2, blocking collectives, sent_and_summed(): lax.all_to_all(parts, axis, split_axis=0, concat_axis=0, tiled=True)  43.7 us
    dot_general x32, matrix products, attend_block(): jnp.dot(raw.astype(jnp.bfloat16), block_values, preferred_element_type=jn...  38.1 us
    dot_general x32, matrix products, attend_block(): lax.dot_general(turned_queries, block_keys, (((1,), (1,)), ((), ())), pre...  37.4 us
    all_gather x1, blocking collectives, stacked_from(): parts = lax.all_gather(parts, axes[k], axis=0, tiled=True)  26.1 us
    unnamed x13, local copies, waits for them, and re-layouts  14.7 us
    all_to_all x1, waiting for transfers between devices, sent_to_all(): lax.all_to_all(jnp.broadcast_to(value[None], (size, *value.shape)), axis,...  12.6 us
  transfers between devices with their start and end apart: 4, of which 2 were waited for; matrix products, arithmetic and copies ran while one was open for 35% of the time, Pallas kernels for 0%

commit v1 on v0

v1 whole, which is shorter than its diff:
```python
import math

import jax
import jax.numpy as jnp
import numpy as np
from jax import lax
from jax.experimental import pallas as pl
from jax.experimental.pallas import tpu as pltpu
from jax.sharding import Mesh
from jax.sharding import PartitionSpec as P

NZ = 8
NY = 8
RING = 8
NX = 4
HEAD = 128
GRID_WIDTH = 64
TOK = 256
TEAM = 4
KTOK = TOK // TEAM
KH = KTOK // 2
ROWS = 32
D = 2048
FFD = 384
EPS = 1e-06
ROPE_BASE = 10000.0
SCALE = HEAD ** (-0.5) * math.log2(math.e)
F32 = jnp.float32
BF16 = jnp.bfloat16
NT = (((1,), (1,)), ((), ()))


def rope_tables():
    quarter = HEAD // 4
    inverse = ROPE_BASE ** (-np.arange(quarter, dtype=np.float64) * 2.0 / (HEAD // 2))
    rows = np.arange(NZ * NY * TOK // GRID_WIDTH, dtype=np.float64)[:, None] * inverse
    cols = np.arange(GRID_WIDTH, dtype=np.float64)[:, None] * inverse

    def half(angles):
        return (
            np.concatenate([np.cos(angles), np.cos(angles)], axis=1),
            np.concatenate([-np.sin(angles), np.sin(angles)], axis=1),
        )

    rc, rs = half(rows)
    cc, cs = half(cols)
    left = lambda a: np.concatenate([a, np.zeros_like(a)], axis=1).astype(np.float32)
    right = lambda a: np.concatenate([np.zeros_like(a), a], axis=1).astype(np.float32)
    return left(rc), left(rs), right(cc), right(cs)


def normalize(x, gain):
    return x * lax.rsqrt(jnp.mean(x * x, axis=-1, keepdims=True) + EPS) * gain


def turn(x, cosine, sine):
    lane = lax.broadcasted_iota(jnp.int32, x.shape, 1)
    ahead = pltpu.roll(x, HEAD - 32, 1)
    behind = pltpu.roll(x, 32, 1)
    partner = jnp.where((lane // 32) % 2 == 0, ahead, behind)
    return x * cosine + partner * sine


def layer_kernel(
    q_ref, k_ref, v_ref, qg_ref, kg_ref, res_ref, ow_hbm, ng_ref, gate_ref, up_ref, down_ref,
    rc_ref, rs_ref, cc_ref, cs_ref,
    out_ref,
    qbuf, kv0, kv1, w, wp, ow, acc, peak, osend, orecv, att, nbuf, mid, psend, pown, precv,
    q_s, q_r, ka_s, ka_r, wa_s, wa_r, kb_s, kb_r, wb_s, wb_r, wr_s, wr_r,
    ow_l, ow_s, ow_r, o_s, o_r, n_s, n_r, p_s, p_r,
):
    z = lax.axis_index("z")
    y = lax.axis_index("y")
    x = lax.axis_index("x")
    c = lax.axis_index("c")
    tp = x * 2 + c
    team = x // 2
    j = lax.rem(x, 2) * 2 + c
    s = z * NY + y
    pos = (z, y)
    axis = ("z", "y")

    def wrap(v, n=RING):
        return lax.rem(v + n, n)

    def tp_id(i):
        return {"x": i // 2, "c": lax.rem(i, 2)}

    own_ow = pltpu.make_async_copy(ow_hbm, ow.at[tp], ow_l)
    own_ow.start()

    barrier = pltpu.get_barrier_semaphore()

    def greet(d, carry):
        pl.semaphore_signal(barrier, inc=1, device_id={"z": wrap(z + d)})
        pl.semaphore_signal(barrier, inc=1, device_id={"y": wrap(y + d)})
        pl.semaphore_signal(barrier, inc=1, device_id=tp_id(wrap(tp + d)))
        return carry

    lax.fori_loop(1, RING, greet, 0)

    k_rows = k_ref[pl.ds(pl.multiple_of(j * KTOK, KTOK), KTOK), :].astype(F32)
    v_rows = v_ref[pl.ds(pl.multiple_of(j * KTOK, KTOK), KTOK), :].astype(F32)
    kk = jnp.where(team == 0, k_rows[:, :HEAD], k_rows[:, HEAD:])
    vv = jnp.where(team == 0, v_rows[:, :HEAD], v_rows[:, HEAD:]).astype(BF16)
    cosine = rc_ref[pl.ds(s * 4 + j, 1), :] + cc_ref[...]
    sine = rs_ref[pl.ds(s * 4 + j, 1), :] + cs_ref[...]
    kk = turn(normalize(kk, kg_ref[...]), cosine, sine).astype(BF16)
    kv0[z, 0, y] = kk[:KH]
    kv0[z, 1, y] = vv[:KH]
    kv1[y, 0, z] = kk[KH:]
    kv1[y, 1, z] = vv[KH:]
    for r in range(4):
        part = slice(r * GRID_WIDTH, (r + 1) * GRID_WIDTH)
        cosine = rc_ref[pl.ds(s * 4 + r, 1), :] + cc_ref[...]
        sine = rs_ref[pl.ds(s * 4 + r, 1), :] + cs_ref[...]
        qq = turn(normalize(q_ref[part, :].astype(F32), qg_ref[...]), cosine, sine)
        qbuf[j, part] = (qq * SCALE).astype(BF16)
    w[0, z, y] = gate_ref[...].reshape(2, 16, FFD)
    w[1, z, y] = up_ref[...].reshape(2, 16, FFD)
    row = lax.broadcasted_iota(jnp.int32, (32, 32), 0)
    col = lax.broadcasted_iota(jnp.int32, (32, 32), 1)
    eye = jnp.where(row == col, 1.0, 0.0).astype(BF16)
    down_t = lax.dot_general(eye, down_ref[...], NT, preferred_element_type=F32)
    w[2, z, y] = down_t.astype(BF16).reshape(2, 16, FFD)
    peak[...] = jnp.full(peak.shape, -1e30, F32)
    acc[...] = jnp.zeros(acc.shape, F32)

    pl.semaphore_wait(barrier, 21)

    def remote(ref, dst, ss, rs, dev):
        return pltpu.make_async_remote_copy(
            src_ref=ref, dst_ref=dst, send_sem=ss, recv_sem=rs,
            device_id=dev, device_id_type=pl.DeviceIdType.MESH,
        )

    def kva(h, d):
        ref = kv0.at[z, :, y] if h == 0 else kv1.at[y, :, z]
        dev = {"y": wrap(y + d)} if h == 0 else {"z": wrap(z + d)}
        return remote(ref, ref, ka_s.at[h, d - 1], ka_r.at[h, d - 1], dev)

    def kva_in(h, d):
        ref = kv0.at[z, :, wrap(y - d)] if h == 0 else kv1.at[y, :, wrap(z - d)]
        return remote(ref, ref, ka_s.at[h, d - 1], ka_r.at[h, d - 1], {"y": y})

    def wa(h, d):
        ref = w.at[:, z, y, h]
        dev = {"y": wrap(y + d)} if h == 0 else {"z": wrap(z + d)}
        return remote(ref, ref, wa_s.at[h, d - 1], wa_r.at[h, d - 1], dev)

    def wa_in(h, d):
        ref = w.at[:, z, wrap(y - d), 0] if h == 0 else w.at[:, wrap(z - d), y, 1]
        return remote(ref, ref, wa_s.at[h, d - 1], wa_r.at[h, d - 1], {"y": y})

    def each(fn):
        def body(d, carry):
            fn(d)
            return carry

        lax.fori_loop(1, RING, body, 0)

    def start_kva(d):
        kva(0, d).start()
        kva(1, d).start()

    each(start_kva)

    def qcopy(d):
        other = team * TEAM + lax.rem(j + d, TEAM)
        return remote(qbuf.at[j], qbuf.at[j], q_s.at[d - 1], q_r.at[d - 1], tp_id(other))

    def qcopy_in(d):
        ref = qbuf.at[lax.rem(j - d + TEAM, TEAM)]
        return remote(ref, ref, q_s.at[d - 1], q_r.at[d - 1], tp_id(tp))

    for d in range(1, TEAM):
        qcopy(d).start()

    right_x = {"x": wrap(x + 1, NX)}
    left_x = {"x": wrap(x - 1, NX)}
    partner = {"c": 1 - c}
    tl = wrap(x - 1, NX) * 2 + c
    tr = wrap(x + 1, NX) * 2 + c
    far = wrap(x + 2, NX) * 2 + c

    def head_ref(i, part=None):
        if part is None:
            return ow.at[i]
        return ow.at[i, pl.ds(part * 64, 64)]

    def owcopy(n, ref, dev):
        return remote(ref, ref, ow_s.at[n], ow_r.at[n], dev)

    ow_out = [
        owcopy(0, head_ref(tp), right_x),
        owcopy(1, head_ref(tp), left_x),
        owcopy(2, head_ref(tp), partner),
        owcopy(3, head_ref(tl, 0), right_x),
        owcopy(4, head_ref(tr, 1), left_x),
        owcopy(5, head_ref(tl), partner),
        owcopy(6, head_ref(tr), partner),
        owcopy(7, head_ref(far, 0), partner),
        owcopy(8, head_ref(far, 1), partner),
    ]
    flip = 1 - 2 * c
    ow_in = [
        owcopy(0, head_ref(tl), right_x),
        owcopy(1, head_ref(tr), left_x),
        owcopy(2, head_ref(tp + flip), partner),
        owcopy(3, head_ref(far, 0), right_x),
        owcopy(4, head_ref(far, 1), left_x),
        owcopy(5, head_ref(tl + flip), partner),
        owcopy(6, head_ref(tr + flip), partner),
        owcopy(7, head_ref(far + flip, 0), partner),
        owcopy(8, head_ref(far + flip, 1), partner),
    ]
    own_ow.wait()

    def start_wa(d):
        wa(0, d).start()
        wa(1, d).start()

    each(start_wa)
    for n in range(3):
        ow_out[n].start()

    def kvb(h, d, k, m, incoming):
        shift = (k if incoming else k - 1) * (-1 if d == 0 else 1)
        buf = kv0 if h == 0 else kv1
        ref = buf.at[wrap(pos[h] + shift), m]
        dev = {axis[h]: wrap(pos[h] + (1 if d == 0 else -1))}
        return remote(ref, ref, kb_s.at[h, d, k - 1, m], kb_r.at[h, d, k - 1, m], dev)

    def kv_steps(k):
        return [(h, d, m) for m in range(2) for h in range(2) for d in range(2) if k < 4 or d == m]

    def kv_send(k):
        for h, d, m in kv_steps(k):
            if k > 1:
                kvb(h, d, k - 1, m, True).wait_recv()
            kvb(h, d, k, m, False).start()
        if k == 4:
            for h, d, m in kv_steps(3):
                if d != m:
                    kvb(h, d, 3, m, True).wait_recv()

    def w_block(h, b, m, lo, hi):
        if h == 0:
            return lambda buf: buf.at[m, b, lo:hi, 0]
        return lambda buf: buf.at[m, lo:hi, b, 1]

    def wb(h, d, k, m, incoming):
        shift = (k if incoming else k - 1) * (-1 if d == 0 else 1)
        lo, hi = (0, RING) if k < 4 else ((0, 4) if d == 0 else (4, RING))
        ref = w_block(h, wrap(pos[h] + shift), m, lo, hi)(w)
        dev = {axis[h]: wrap(pos[h] + (1 if d == 0 else -1))}
        return remote(ref, ref, wb_s.at[h, d, k - 1, m], wb_r.at[h, d, k - 1, m], dev)

    def hand_over(h, d, k, m):
        shift = k * (-1 if d == 0 else 1)
        lo, hi = (0, RING) if k < 4 else ((0, 4) if d == 0 else (4, RING))
        pick = w_block(h, wrap(pos[h] + shift), m, lo, hi)
        remote(pick(w), pick(wp), wr_s.at[m], wr_r.at[m], partner).start()

    def pump(p):
        k, m = p // 3 + 1, p % 3
        for h in range(2):
            for d in range(2):
                if k > 1:
                    wb(h, d, k - 1, m, True).wait_recv()
                if k <= 4:
                    wb(h, d, k, m, False).start()
        for h in range(2):
            for d in range(2):
                if k > 1:
                    hand_over(h, d, k - 1, m)
                elif d == 0:
                    hand_over(h, 0, 0, m)

    ones = jnp.ones((1, HEAD), BF16)

    def attend(blocks):
        keys = jnp.concatenate([buf[b, 0].reshape(256, HEAD) for buf, b in blocks], axis=0)
        vals = jnp.concatenate([buf[b, 1].reshape(256, HEAD) for buf, b in blocks], axis=0)
        wide = keys.shape[0]
        vals = jnp.concatenate([vals, jnp.broadcast_to(ones, vals.shape)], axis=1)

        def one_head(h, carry):
            scores = lax.dot_general(qbuf[h], keys, NT, preferred_element_type=F32)
            old = peak[h]
            new = jnp.maximum(old, jnp.max(scores, axis=1, keepdims=True))
            factor = jnp.exp2(old - new)
            peak[h] = new
            raw = jnp.exp2(scores - jnp.concatenate([new] * (wide // HEAD), axis=1)).astype(BF16)
            update = jnp.dot(raw, vals, preferred_element_type=F32)
            acc[h] = acc[h] * jnp.concatenate([factor, factor], axis=1) + update
            return carry

        lax.fori_loop(0, TEAM, one_head, 0)

    def wait_kva(d):
        kva_in(0, d).wait_recv()
        kva_in(1, d).wait_recv()

    def wait_wa(d):
        wa_in(0, d).wait_recv()
        wa_in(1, d).wait_recv()

    each(wait_kva)
    kv_send(1)
    for d in range(1, TEAM):
        qcopy_in(d).wait_recv()
    attend([(kv0, z), (kv1, y)])
    kv_send(2)
    each(wait_wa)
    pump(0)
    attend([(kv0, wrap(z - 1)), (kv0, wrap(z + 1)), (kv1, wrap(y - 1)), (kv1, wrap(y + 1))])
    kv_send(3)
    pump(1)
    attend([(kv0, wrap(z - 2)), (kv0, wrap(z + 2)), (kv1, wrap(y - 2)), (kv1, wrap(y + 2))])
    kv_send(4)
    pump(2)
    ow_in[0].wait_recv()
    ow_out[3].start()
    ow_in[1].wait_recv()
    ow_out[4].start()
    ow_out[5].start()
    ow_out[6].start()
    attend([(kv0, wrap(z - 3)), (kv0, wrap(z + 3)), (kv1, wrap(y - 3)), (kv1, wrap(y + 3))])
    for h, d, m in kv_steps(4):
        kvb(h, d, 4, m, True).wait_recv()
    pump(3)
    attend([(kv0, wrap(z + 4)), (kv1, wrap(y + 4))])

    lane = lax.broadcasted_iota(jnp.int32, (TOK, HEAD), 1)
    stats = jnp.zeros((TOK, HEAD), F32)
    for h in range(TEAM):
        total = acc[h, :, HEAD:]
        mean = (acc[h, :, :HEAD] / total).astype(BF16)
        osend[:, :, h * HEAD : (h + 1) * HEAD] = mean.reshape(8, ROWS, HEAD)
        level = peak[h] + jnp.log2(total)
        first = level.astype(BF16).astype(F32)
        second = (level - first).astype(BF16).astype(F32)
        third = level - first - second
        stats = jnp.where(lane == h, first, stats)
        stats = jnp.where(lane == h + 4, second, stats)
        stats = jnp.where(lane == h + 8, third, stats)
    osend[:, :, TEAM * HEAD :] = stats.astype(BF16).reshape(8, ROWS, HEAD)

    def ocopy(d):
        i = wrap(tp + d)
        return remote(osend.at[i], orecv.at[tp], o_s.at[d - 1], o_r.at[d - 1], tp_id(i))

    def ocopy_in(d):
        ref = orecv.at[wrap(tp - d)]
        return remote(ref, ref, o_s.at[d - 1], o_r.at[d - 1], tp_id(tp))

    each(lambda d: ocopy(d).start())
    orecv[tp] = osend[tp]

    ow_in[3].wait_recv()
    ow_out[7].start()
    ow_in[4].wait_recv()
    ow_out[8].start()
    pump(4)
    pump(5)

    each(lambda d: ocopy_in(d).wait_recv())
    for t in range(2):
        for h in range(TEAM):
            levels = []
            for i in range(t * TEAM, (t + 1) * TEAM):
                st = orecv[i, :, TEAM * HEAD :].astype(F32)
                levels.append(st[:, h : h + 1] + st[:, h + 4 : h + 5] + st[:, h + 8 : h + 9])
            top = jnp.maximum(jnp.maximum(levels[0], levels[1]), jnp.maximum(levels[2], levels[3]))
            shares = [jnp.exp2(v - top) for v in levels]
            total = shares[0] + shares[1] + shares[2] + shares[3]
            mixed = jnp.zeros((ROWS, HEAD), F32)
            for i in range(TEAM):
                block = orecv[t * TEAM + i, :, h * HEAD : (h + 1) * HEAD].astype(F32)
                mixed = mixed + block * shares[i]
            at = (t * TEAM + h) * HEAD
            att[:, at : at + HEAD] = (mixed / total).astype(BF16)

    for n in (2, 5, 6, 7, 8):
        ow_in[n].wait_recv()
    projected = jnp.dot(att[...], ow[...].reshape(8 * HEAD, D), preferred_element_type=F32)
    middle = (res_ref[...].astype(F32) + projected).astype(BF16)
    mid[...] = middle
    nbuf[x] = normalize(middle.astype(F32), ng_ref[...]).astype(BF16)

    def ncopy(n, ref, dev):
        return remote(ref, ref, n_s.at[n], n_r.at[n], dev)

    xl, xr, xf = wrap(x - 1, NX), wrap(x + 1, NX), wrap(x + 2, NX)
    n_out = [
        ncopy(0, nbuf.at[x], right_x),
        ncopy(1, nbuf.at[x], left_x),
        ncopy(2, nbuf.at[xl, pl.ds(0, 16)], right_x),
        ncopy(3, nbuf.at[xr, pl.ds(16, 16)], left_x),
    ]
    n_in = [
        ncopy(0, nbuf.at[xl], right_x),
        ncopy(1, nbuf.at[xr], left_x),
        ncopy(2, nbuf.at[xf, pl.ds(0, 16)], right_x),
        ncopy(3, nbuf.at[xf, pl.ds(16, 16)], left_x),
    ]
    n_out[0].start()
    n_out[1].start()
    pump(6)
    pump(7)
    n_in[0].wait_recv()
    n_out[2].start()
    n_in[1].wait_recv()
    n_out[3].start()
    for p in range(8, 15):
        pump(p)
    n_in[2].wait_recv()
    n_in[3].wait_recv()
    normed = nbuf[...].reshape(NX * ROWS, D)

    def all_of(m):
        return remote(w.at[m], wp.at[m], wr_s.at[m], wr_r.at[m], partner)

    def hidden_of(buf):
        gate_part = jnp.dot(normed, buf[0].reshape(D, FFD), preferred_element_type=F32)
        lifted = jnp.dot(normed, buf[1].reshape(D, FFD), preferred_element_type=F32)
        return (gate_part / (1.0 + jnp.exp(-gate_part)) * lifted).astype(BF16)

    hidden = hidden_of(w)
    all_of(0).wait_recv()
    all_of(1).wait_recv()
    hidden_p = hidden_of(wp)
    all_of(2).wait_recv()
    parts = lax.dot_general(hidden, w[2].reshape(D, FFD), NT, preferred_element_type=F32)
    parts = parts + lax.dot_general(hidden_p, wp[2].reshape(D, FFD), NT, preferred_element_type=F32)
    parts = parts.reshape(NX, ROWS, D)
    psend[...] = parts.astype(BF16)
    pown[...] = parts

    def pcopy(d):
        i = wrap(x + d, NX)
        return remote(psend.at[i], precv.at[x], p_s.at[d - 1], p_r.at[d - 1], {"x": i})

    def pcopy_in(d):
        ref = precv.at[wrap(x - d, NX)]
        return remote(ref, ref, p_s.at[d - 1], p_r.at[d - 1], {"x": x})

    for d in (2, 1, 3):
        pcopy(d).start()

    def drain(d):
        for h in range(2):
            kva(h, d).wait_send()
            wa(h, d).wait_send()
        ocopy(d).wait_send()

    each(drain)
    for d in range(1, TEAM):
        qcopy(d).wait_send()
    for copy in ow_out + n_out:
        copy.wait_send()
    for k in range(1, 5):
        for h, d, m in kv_steps(k):
            kvb(h, d, k, m, False).wait_send()
        for h in range(2):
            for d in range(2):
                for m in range(3):
                    wb(h, d, k, m, False).wait_send()
    for m in range(3):
        all_of(m).wait_send()

    total = mid[...].astype(F32) + pown[x]
    for d in (1, 3, 2):
        pcopy_in(d).wait_recv()
        total = total + precv[wrap(x - d, NX)].astype(F32)
    out_ref[...] = total.astype(BF16)
    for d in range(1, NX):
        pcopy(d).wait_send()


def local(
    queries, keys, values, query_gain, key_gain, residual_in, out_weight, norm_gain,
    gate_weight, up_weight, down_weight,
):
    vmem = pl.BlockSpec(memory_space=pltpu.VMEM)
    dma = pltpu.SemaphoreType.DMA
    tables = [jnp.asarray(t) for t in rope_tables()]
    return pl.pallas_call(
        layer_kernel,
        name="layer",
        out_shape=jax.ShapeDtypeStruct((ROWS, D), BF16),
        in_specs=[vmem] * 6 + [pl.BlockSpec(memory_space=pl.ANY)] + [vmem] * 8,
        out_specs=vmem,
        scratch_shapes=[
            pltpu.VMEM((TEAM, TOK, HEAD), BF16),
            pltpu.VMEM((NZ, 2, NY, KH, HEAD), BF16),
            pltpu.VMEM((NY, 2, NZ, KH, HEAD), BF16),
            pltpu.VMEM((3, NZ, NY, 2, 16, FFD), BF16),
            pltpu.VMEM((3, NZ, NY, 2, 16, FFD), BF16),
            pltpu.VMEM((8, HEAD, D), BF16),
            pltpu.VMEM((TEAM, TOK, 2 * HEAD), F32),
            pltpu.VMEM((TEAM, TOK, HEAD), F32),
            pltpu.VMEM((8, ROWS, (TEAM + 1) * HEAD), BF16),
            pltpu.VMEM((8, ROWS, (TEAM + 1) * HEAD), BF16),
            pltpu.VMEM((ROWS, 8 * HEAD), BF16),
            pltpu.VMEM((NX, ROWS, D), BF16),
            pltpu.VMEM((ROWS, D), BF16),
            pltpu.VMEM((NX, ROWS, D), BF16),
            pltpu.VMEM((NX, ROWS, D), F32),
            pltpu.VMEM((NX, ROWS, D), BF16),
            dma((3,)), dma((3,)),
            dma((2, 7)), dma((2, 7)),
            dma((2, 7)), dma((2, 7)),
            dma((2, 2, 4, 2)), dma((2, 2, 4, 2)),
            dma((2, 2, 4, 3)), dma((2, 2, 4, 3)),
            dma((3,)), dma((3,)),
            dma, dma((9,)), dma((9,)),
            dma((7,)), dma((7,)),
            dma((4,)), dma((4,)),
            dma((3,)), dma((3,)),
        ],
        compiler_params=pltpu.CompilerParams(
            collective_id=0, has_side_effects=True, vmem_limit_bytes=56 * 1024 * 1024
        ),
    )(
        queries, keys, values, query_gain.reshape(1, -1), key_gain.reshape(1, -1), residual_in,
        out_weight, norm_gain.reshape(1, -1), gate_weight, up_weight, down_weight, *tables,
    )


def solution(mesh):
    finer = Mesh(mesh.devices.reshape(NZ, NY, NX, 2), ("z", "y", "x", "c"))
    sp, tp = ("z", "y"), ("x", "c")
    in_specs = (
        P(sp, tp),
        P(sp, None),
        P(sp, None),
        P(),
        P(),
        P(sp + tp, None),
        P(tp, None),
        P(),
        P(sp, tp),
        P(sp, tp),
        P(tp, sp),
    )
    return jax.shard_map(
        local, mesh=finer, in_specs=in_specs, out_specs=P(sp + tp, None), check_vma=False
    )
```

time: 301 us -> 84.9 us (0.28)
  waiting for transfers between devices: 92.8 us -> 0 us
  matrix products: 82.6 us -> 0 us
  Pallas kernels: 0 us -> 81.6 us
  blocking collectives: 69.7 us -> 0 us
  local copies, waits for them, and re-layouts: 25 us -> 3.05 us
  between operations: 13.3 us -> 0.01 us
  other arithmetic: 9.95 us -> 0 us
  starting transfers between devices: 4.58 us -> 0 us
    dot_general x67 -> x0, matrix products: 82.6 us -> none  [the longest x32 38.1 us: attend_block(): jnp.dot(raw.astype(jnp.bfloat16), block_values, preferred_element_type=jn...]
    pallas_call x0 -> x1, Pallas kernels: none -> 81.6 us  [local(): pl.pallas_call(layer_kernel, name='layer', out_shape=jax.ShapeDtypeStruct...]
    all_gather x3 -> x0, waiting for transfers between devices: 80.1 us -> none  [the longest x2 80.1 us: side_by_side(): result = lax.all_gather(both, axis, axis=dim, tiled=True)]
    all_to_all x2 -> x0, blocking collectives: 43.7 us -> none  [sent_and_summed(): lax.all_to_all(parts, axis, split_axis=0, concat_axis=0, tiled=True)]
    all_gather x1 -> x0, blocking collectives: 26.1 us -> none  [stacked_from(): parts = lax.all_gather(parts, axes[k], axis=0, tiled=True)]
    all_to_all x1 -> x0, waiting for transfers between devices: 12.6 us -> none  [sent_to_all(): lax.all_to_all(jnp.broadcast_to(value[None], (size, *value.shape)), axis,...]
    unnamed x13 -> x2, local copies, waits for them, and re-layouts: 14.7 us -> 3.05 us
    split x1 -> x0, local copies, waits for them, and re-layouts: 5.8 us -> none  [side_by_side(): jnp.split(result, [sum(widths[:k]) for k in range(1, len(widths))], axis=...]
  transfers between devices with their start and end apart: 4 -> 0, of which waited for: 2 -> 0; matrix products, arithmetic and copies ran while one was open for 35% -> 0% of each run, Pallas kernels for 0% -> 0%
where the time goes in v1:
time: 84.9 us; the launch traced here: 84.7 us
  Pallas kernels  81.6 us (96%)
  local copies, waits for them, and re-layouts  3.05 us (4%)
    pallas_call x1, Pallas kernels, local(): pl.pallas_call(layer_kernel, name='layer', out_shape=jax.ShapeDtypeStruct...  81.6 us
    unnamed x2, local copies, waits for them, and re-layouts  3.05 us

profile of v1, /device:TPU:1, one launch (start us, length us, event | category | flops | bytes accessed | tf_op | source)
XLA Modules:
  0.0 84.7 jit_solution(13054192435470258456)
XLA Ops:
  0.0 1.5 %copy.16.down_ref = bf16[384,32]{1,0:T(8,128)(2,1)} copy(bf16[384,32]{0,1:T(8,128)(2,1)} %param.25) | data formatting | bytes 49152 | tf_op args[10]
  1.5 81.6 %layer.1 = bf16[32,2048]{1,0:T(8,128)(2,1)} custom-call(bf16[256,128]{1,0:T(8,128)(2,1)} %q_ref.1, bf16[256,256]{1,0:T(8,128)(2,1)} %k_ref.1, bf16[256,256]{1,0:T(8,128)(2,1)} %v_ref.1, f32[1,128]{1,0:T(1,128)} %bitcast.4, f32[1,128]{1,0:T(1,128)} %bitcast.5, bf16[32,2048]{1,0:T(8,128)(2,1)} %res_ref.1, bf16[128,2048]{1,0:T(8,128)(2,1)} %ow_hbm.1, ...), custom_call_target="tpu_custom_call" | custom-call | tf_op jit(solution)/shard_map/layer/pallas_call | solution.py:489
  83.1 1.6 %copy.18 = bf16[32,2048]{1,0:T(8,128)(2,1)} copy(bf16[32,2048]{1,0:T(8,128)(2,1)} %layer.1) | data formatting | bytes 262144

commit v2 on v1

v2 whole, which is shorter than its diff:
```python
import math

import jax
import jax.numpy as jnp
import numpy as np
from jax import lax
from jax.experimental import pallas as pl
from jax.experimental.pallas import tpu as pltpu
from jax.sharding import Mesh
from jax.sharding import PartitionSpec as P

NZ = 8
NY = 8
RING = 8
NX = 4
HEAD = 128
GRID_WIDTH = 64
TOK = 256
TEAM = 4
KTOK = TOK // TEAM
KH = KTOK // 2
ROWS = 32
D = 2048
FFD = 384
EPS = 1e-06
ROPE_BASE = 10000.0
SCALE = HEAD ** (-0.5) * math.log2(math.e)
F32 = jnp.float32
BF16 = jnp.bfloat16
NT = (((1,), (1,)), ((), ()))
FAR_FIRST = (4, 3, 5, 2, 6, 1, 7)


def rope_tables():
    quarter = HEAD // 4
    inverse = ROPE_BASE ** (-np.arange(quarter, dtype=np.float64) * 2.0 / (HEAD // 2))
    rows = np.arange(NZ * NY * TOK // GRID_WIDTH, dtype=np.float64)[:, None] * inverse
    cols = np.arange(GRID_WIDTH, dtype=np.float64)[:, None] * inverse

    def half(angles):
        return (
            np.concatenate([np.cos(angles), np.cos(angles)], axis=1),
            np.concatenate([-np.sin(angles), np.sin(angles)], axis=1),
        )

    rc, rs = half(rows)
    cc, cs = half(cols)
    rc, rs = rc.reshape(-1, 4, HEAD // 2), rs.reshape(-1, 4, HEAD // 2)
    left = lambda a: np.concatenate([a, np.zeros_like(a)], axis=-1).astype(np.float32)
    right = lambda a: np.concatenate([np.zeros_like(a), a], axis=-1).astype(np.float32)
    return np.stack([left(rc), left(rs)], axis=1), np.stack([right(cc), right(cs)])


def normalize(x, gain):
    return x * lax.rsqrt(jnp.mean(x * x, axis=-1, keepdims=True) + EPS) * gain


def turn(x, cosine, sine):
    lane = lax.broadcasted_iota(jnp.int32, x.shape, 1)
    ahead = pltpu.roll(x, HEAD - 32, 1)
    behind = pltpu.roll(x, 32, 1)
    partner = jnp.where((lane // 32) % 2 == 0, ahead, behind)
    return x * cosine + partner * sine


def layer_kernel(
    q_hbm, k_hbm, v_hbm, qg_hbm, kg_hbm, res_hbm, ow_hbm, ng_hbm, gate_hbm, up_hbm, down_hbm,
    row_hbm, col_hbm,
    out_ref,
    q_ref, k_ref, qg_ref, kg_ref, res_ref, ng_ref, row_ref, col_ref,
    qbuf, kv0, kv1, w, wp, ow, acc, peak, osend, orecv, att, nbuf, mid, psend, pown, precv, pfar, pmix,
    in_s, q_s, q_r, ka_s, ka_r, wa_s, wa_r, kb_s, kb_r, wb_s, wb_r, wr_s, wr_r,
    ow_s, ow_r, o_s, o_r, n_s, n_r, p_s, p_r,
):
    z = lax.axis_index("z")
    y = lax.axis_index("y")
    x = lax.axis_index("x")
    c = lax.axis_index("c")
    tp = x * 2 + c
    team = x // 2
    j = lax.rem(x, 2) * 2 + c
    s = z * NY + y
    pos = (z, y)
    axis = ("z", "y")

    def wrap(v, n=RING):
        return lax.rem(v + n, n)

    def tp_id(i):
        return {"x": i // 2, "c": lax.rem(i, 2)}

    barrier = pltpu.get_barrier_semaphore()

    def greet(d, carry):
        pl.semaphore_signal(barrier, inc=1, device_id={"z": wrap(z + d)})
        pl.semaphore_signal(barrier, inc=1, device_id={"y": wrap(y + d)})
        pl.semaphore_signal(barrier, inc=1, device_id=tp_id(wrap(tp + d)))
        return carry

    lax.fori_loop(1, RING, greet, 0)

    lanes = pl.ds(pl.multiple_of(team * HEAD, HEAD), HEAD)

    def key_rows(half):
        return pl.ds(pl.multiple_of(j * KTOK + half * KH, KH), KH)

    loads = [
        (k_hbm.at[pl.ds(pl.multiple_of(j * KTOK, KTOK), KTOK), lanes], k_ref),
        (row_hbm.at[s], row_ref),
        (col_hbm, col_ref),
        (kg_hbm, kg_ref),
        (q_hbm, q_ref),
        (qg_hbm, qg_ref),
        (ow_hbm, ow.at[tp]),
        (res_hbm, res_ref),
        (ng_hbm, ng_ref),
        (v_hbm.at[key_rows(0), lanes], kv0.at[z, 1, y]),
        (v_hbm.at[key_rows(1), lanes], kv1.at[y, 1, z]),
        (gate_hbm, w.at[0, z, y]),
        (up_hbm, w.at[1, z, y]),
        (down_hbm, w.at[2, z, y]),
    ]
    sems = [in_s.at[n] for n in (0, 1, 2, 3, 4, 5, 6, 7, 8, 9, 9, 10, 10, 10)]
    loads = [pltpu.make_async_copy(a, b, m) for (a, b), m in zip(loads, sems)]

    def landed(ref, sem):
        pltpu.make_async_copy(ref, ref, sem).wait()

    for load in loads:
        load.start()

    for load in loads[:4]:
        load.wait()
    cosine = row_ref[0, pl.ds(j, 1), :] + col_ref[0]
    sine = row_ref[1, pl.ds(j, 1), :] + col_ref[1]
    kk = k_ref[...].astype(F32)
    kk = turn(normalize(kk, kg_ref[...]), cosine, sine).astype(BF16)
    kv0[z, 0, y] = kk[:KH]
    kv1[y, 0, z] = kk[KH:]
    landed(kv0.at[z, 1, 0:2], in_s.at[9])
    pl.semaphore_wait(barrier, 21)

    partner = {"c": 1 - c}

    def remote(ref, dst, ss, rs, dev):
        return pltpu.make_async_remote_copy(
            src_ref=ref, dst_ref=dst, send_sem=ss, recv_sem=rs,
            device_id=dev, device_id_type=pl.DeviceIdType.MESH,
        )

    def arrived(ref, sem):
        remote(ref, ref, sem, sem, partner).wait_recv()

    def sent(ref, sem):
        remote(ref, ref, sem, sem, partner).wait_send()

    def kva(h, d):
        ref = kv0.at[z, :, y] if h == 0 else kv1.at[y, :, z]
        dev = {"y": wrap(y + d)} if h == 0 else {"z": wrap(z + d)}
        return remote(ref, ref, ka_s.at[h], ka_r.at[h], dev)

    def wa(h, d, part):
        pick = slice(0, 2) if part == 0 else slice(2, 3)
        ref = w.at[pick, z, y, h]
        dev = {"y": wrap(y + d)} if h == 0 else {"z": wrap(z + d)}
        return remote(ref, ref, wa_s.at[h], wa_r.at[part, h], dev)

    def w_first(part):
        for d in FAR_FIRST:
            wa(0, d, part).start()
            wa(1, d, part).start()

    def w_first_in(part):
        pick = slice(0, 2) if part == 0 else slice(2, 3)
        arrived(w.at[pick, z, 0:7, 0], wa_r.at[part, 0])
        arrived(w.at[pick, 0:7, y, 1], wa_r.at[part, 1])

    def start_kva(d):
        kva(0, d).start()
        kva(1, d).start()

    for d in FAR_FIRST:
        start_kva(d)
    landed(w.at[:, z, y], in_s.at[10])
    w_first(0)

    loads[4].wait()
    loads[5].wait()
    for r in range(4):
        part = slice(r * GRID_WIDTH, (r + 1) * GRID_WIDTH)
        cosine = row_ref[0, r : r + 1, :] + col_ref[0]
        sine = row_ref[1, r : r + 1, :] + col_ref[1]
        qq = turn(normalize(q_ref[part, :].astype(F32), qg_ref[...]), cosine, sine)
        qbuf[j, part] = (qq * SCALE).astype(BF16)
    peak[...] = jnp.full(peak.shape, -1e30, F32)
    acc[...] = jnp.zeros(acc.shape, F32)

    def qcopy(d):
        other = team * TEAM + lax.rem(j + d, TEAM)
        return remote(qbuf.at[j], qbuf.at[j], q_s, q_r, tp_id(other))

    for d in range(1, TEAM):
        qcopy(d).start()

    right_x = {"x": wrap(x + 1, NX)}
    left_x = {"x": wrap(x - 1, NX)}
    tl = wrap(x - 1, NX) * 2 + c
    tr = wrap(x + 1, NX) * 2 + c
    far = wrap(x + 2, NX) * 2 + c

    def head_ref(i, part=None):
        if part is None:
            return ow.at[i]
        return ow.at[i, pl.ds(part * 64, 64)]

    def owcopy(n, ref, dev):
        return remote(ref, ref, ow_s, ow_r.at[n], dev)

    ow_out = [
        owcopy(0, head_ref(tp), right_x),
        owcopy(1, head_ref(tp), left_x),
        owcopy(4, head_ref(tp), partner),
        owcopy(2, head_ref(tl, 0), right_x),
        owcopy(3, head_ref(tr, 1), left_x),
        owcopy(4, head_ref(tl), partner),
        owcopy(4, head_ref(tr), partner),
        owcopy(4, head_ref(far, 0), partner),
        owcopy(4, head_ref(far, 1), partner),
    ]
    ow_in = [
        owcopy(0, head_ref(tl), right_x),
        owcopy(1, head_ref(tr), left_x),
        owcopy(2, head_ref(far, 0), right_x),
        owcopy(3, head_ref(far, 1), left_x),
    ]
    loads[6].wait()

    for n in range(3):
        ow_out[n].start()

    def kvb(h, d, k, m):
        shift = (k - 1) * (-1 if d == 0 else 1)
        buf = kv0 if h == 0 else kv1
        ref = buf.at[wrap(pos[h] + shift), m]
        dev = {axis[h]: wrap(pos[h] + (1 if d == 0 else -1))}
        return remote(ref, ref, kb_s.at[h], kb_r.at[k - 1], dev)

    def kv_steps(k):
        return [(h, d, m) for m in range(2) for h in range(2) for d in range(2) if k < 4 or d == m]

    def kv_send(k):
        if k > 1:
            arrived(kv0.at[0:4], kb_r.at[k - 2])
        for h, d, m in kv_steps(k):
            kvb(h, d, k, m).start()

    def w_block(h, b, m, lo, hi):
        if h == 0:
            return lambda buf: buf.at[m, b, lo:hi, 0]
        return lambda buf: buf.at[m, lo:hi, b, 1]

    def wb(h, d, k, m):
        shift = (k - 1) * (-1 if d == 0 else 1)
        lo, hi = (0, RING) if k < 4 else ((0, 4) if d == 0 else (4, RING))
        ref = w_block(h, wrap(pos[h] + shift), m, lo, hi)(w)
        dev = {axis[h]: wrap(pos[h] + (1 if d == 0 else -1))}
        return remote(ref, ref, wb_s, wb_r.at[k - 1, m], dev)

    def hand_over(h, d, k, m):
        shift = k * (-1 if d == 0 else 1)
        lo, hi = (0, RING) if k < 4 else ((0, 4) if d == 0 else (4, RING))
        pick = w_block(h, wrap(pos[h] + shift), m, lo, hi)
        remote(pick(w), pick(wp), wr_s, wr_r.at[m], partner).start()

    def pump(k, m):
        if k > 1:
            arrived(w.at[m, 0 : 2 if k < 5 else 1], wb_r.at[k - 2, m])
        if k <= 4:
            for h in range(2):
                for d in range(2):
                    wb(h, d, k, m).start()
        for h in range(2):
            for d in range(2):
                if k > 1:
                    hand_over(h, d, k - 1, m)
                elif d == 0:
                    hand_over(h, 0, 0, m)

    ones = jnp.ones((1, HEAD), BF16)

    def attend(blocks):
        keys = jnp.concatenate([buf[b, 0].reshape(256, HEAD) for buf, b in blocks], axis=0)
        vals = jnp.concatenate([buf[b, 1].reshape(256, HEAD) for buf, b in blocks], axis=0)
        wide = keys.shape[0]
        vals = jnp.concatenate([vals, jnp.broadcast_to(ones, vals.shape)], axis=1)

        def scores_of(h):
            return lax.dot_general(qbuf[h], keys, NT, preferred_element_type=F32)

        scores = scores_of(0)
        for h in range(TEAM):
            later = scores_of(h + 1) if h + 1 < TEAM else None
            old = peak[h]
            new = jnp.maximum(old, jnp.max(scores, axis=1, keepdims=True))
            factor = jnp.exp2(old - new)
            peak[h] = new
            raw = jnp.exp2(scores - jnp.concatenate([new] * (wide // HEAD), axis=1)).astype(BF16)
            update = jnp.dot(raw, vals, preferred_element_type=F32)
            acc[h] = acc[h] * jnp.concatenate([factor, factor], axis=1) + update
            scores = later

    arrived(kv0.at[0, :, 0:7], ka_r.at[0])
    arrived(kv0.at[0, :, 0:7], ka_r.at[1])
    kv_send(1)
    arrived(qbuf.at[0:3], q_r)
    w_first_in(0)
    pump(1, 0)
    attend([(kv0, z), (kv1, y)])
    kv_send(2)
    pump(1, 1)
    w_first(1)
    attend([(kv0, wrap(z - 1)), (kv0, wrap(z + 1)), (kv1, wrap(y - 1)), (kv1, wrap(y + 1))])
    kv_send(3)
    pump(2, 0)
    ow_in[0].wait_recv()
    ow_out[3].start()
    ow_in[1].wait_recv()
    ow_out[4].start()
    ow_out[5].start()
    ow_out[6].start()
    attend([(kv0, wrap(z - 2)), (kv0, wrap(z + 2)), (kv1, wrap(y - 2)), (kv1, wrap(y + 2))])
    kv_send(4)
    pump(2, 1)
    attend([(kv0, wrap(z - 3)), (kv0, wrap(z + 3)), (kv1, wrap(y - 3)), (kv1, wrap(y + 3))])
    w_first_in(1)
    pump(1, 2)
    arrived(kv0.at[0:2], kb_r.at[3])
    attend([(kv0, wrap(z + 4)), (kv1, wrap(y + 4))])
    pump(3, 0)

    lane = lax.broadcasted_iota(jnp.int32, (TOK, HEAD), 1)
    stats = jnp.zeros((TOK, HEAD), F32)
    for h in range(TEAM):
        total = acc[h, :, HEAD:]
        mean = (acc[h, :, :HEAD] / total).astype(BF16)
        osend[:, :, h * HEAD : (h + 1) * HEAD] = mean.reshape(8, ROWS, HEAD)
        level = peak[h] + jnp.log2(total)
        first = level.astype(BF16).astype(F32)
        second = (level - first).astype(BF16).astype(F32)
        third = level - first - second
        stats = jnp.where(lane == h, first, stats)
        stats = jnp.where(lane == h + 4, second, stats)
        stats = jnp.where(lane == h + 8, third, stats)
    osend[:, :, TEAM * HEAD :] = stats.astype(BF16).reshape(8, ROWS, HEAD)

    def ocopy(d):
        i = wrap(tp + d)
        return remote(osend.at[i], orecv.at[tp], o_s, o_r, tp_id(i))

    for d in (4, 3, 5, 2, 6, 1, 7):
        ocopy(d).start()
    orecv[tp] = osend[tp]

    pump(3, 1)
    ow_in[2].wait_recv()
    ow_out[7].start()
    ow_in[3].wait_recv()
    ow_out[8].start()
    pump(2, 2)

    arrived(orecv.at[0:7], o_r)
    for t in range(2):
        for h in range(TEAM):
            levels = []
            for i in range(t * TEAM, (t + 1) * TEAM):
                st = orecv[i, :, TEAM * HEAD :].astype(F32)
                levels.append(st[:, h : h + 1] + st[:, h + 4 : h + 5] + st[:, h + 8 : h + 9])
            top = jnp.maximum(jnp.maximum(levels[0], levels[1]), jnp.maximum(levels[2], levels[3]))
            shares = [jnp.exp2(v - top) for v in levels]
            total = shares[0] + shares[1] + shares[2] + shares[3]
            mixed = jnp.zeros((ROWS, HEAD), F32)
            for i in range(TEAM):
                block = orecv[t * TEAM + i, :, h * HEAD : (h + 1) * HEAD].astype(F32)
                mixed = mixed + block * shares[i]
            at = (t * TEAM + h) * HEAD
            att[:, at : at + HEAD] = (mixed / total).astype(BF16)

    arrived(ow.at[0:4], ow_r.at[4])
    loads[7].wait()
    loads[8].wait()
    projected = jnp.dot(att[...], ow[...].reshape(8 * HEAD, D), preferred_element_type=F32)
    middle = (res_ref[...].astype(F32) + projected).astype(BF16)
    mid[...] = middle
    nbuf[x] = normalize(middle.astype(F32), ng_ref[...]).astype(BF16)

    def ncopy(n, ref, dev):
        return remote(ref, ref, n_s, n_r.at[min(n, 2)], dev)

    xl, xr, xf = wrap(x - 1, NX), wrap(x + 1, NX), wrap(x + 2, NX)
    low, high = pl.ds(0, 16), pl.ds(16, 16)
    n_out = [
        ncopy(0, nbuf.at[x, low], right_x),
        ncopy(1, nbuf.at[x, high], left_x),
        ncopy(2, nbuf.at[x, high], right_x),
        ncopy(3, nbuf.at[x, low], left_x),
        ncopy(4, nbuf.at[xl, low], right_x),
        ncopy(5, nbuf.at[xr, high], left_x),
    ]
    n_in = [
        ncopy(0, nbuf.at[xl, low], right_x),
        ncopy(1, nbuf.at[xr, high], left_x),
    ]
    for copy in n_out[:4]:
        copy.start()
    pump(4, 0)
    n_in[0].wait_recv()
    n_out[4].start()
    n_in[1].wait_recv()
    n_out[5].start()
    pump(4, 1)
    pump(3, 2)
    pump(5, 0)
    pump(5, 1)
    arrived(nbuf.at[0:2], n_r.at[2])
    normed = nbuf[...].reshape(NX * ROWS, D)

    def all_of(m):
        return remote(w.at[m], wp.at[m], wr_s, wr_r.at[m], partner)

    def hidden_of(buf):
        gate_part = jnp.dot(normed, buf[0].reshape(D, FFD), preferred_element_type=F32)
        lifted = jnp.dot(normed, buf[1].reshape(D, FFD), preferred_element_type=F32)
        return (gate_part / (1.0 + jnp.exp(-gate_part)) * lifted).astype(BF16)

    hidden = hidden_of(w)
    pump(4, 2)
    all_of(0).wait_recv()
    all_of(1).wait_recv()
    hidden_p = hidden_of(wp)
    pump(5, 2)
    all_of(2).wait_recv()
    parts = lax.dot_general(hidden, w[2].reshape(D, FFD), NT, preferred_element_type=F32)
    parts = parts + lax.dot_general(hidden_p, wp[2].reshape(D, FFD), NT, preferred_element_type=F32)
    parts = parts.reshape(NX, ROWS, D)
    psend[...] = parts.astype(BF16)
    pown[...] = parts

    def pcopy(n, src, dst, dev):
        return remote(src, dst, p_s, p_r.at[min(n, 2)], dev)

    p_copies = [
        pcopy(0, psend.at[xf, low], pfar.at[0], right_x),
        pcopy(1, psend.at[xf, high], pfar.at[1], left_x),
        pcopy(2, psend.at[xr, high], precv.at[0, high], right_x),
        pcopy(3, psend.at[xl, low], precv.at[1, low], left_x),
        pcopy(4, pmix.at[0], precv.at[0, low], right_x),
        pcopy(5, pmix.at[1], precv.at[1, high], left_x),
    ]
    for copy in p_copies[:4]:
        copy.start()
    p_copies[0].wait_recv()
    pmix[0] = (pown[xr, low] + pfar[0].astype(F32)).astype(BF16)
    p_copies[4].start()
    p_copies[1].wait_recv()
    pmix[1] = (pown[xl, high] + pfar[1].astype(F32)).astype(BF16)
    p_copies[5].start()

    def drain():
        for h in range(2):
            sent(kv0.at[0, :, 0:7], ka_s.at[h])
            sent(w.at[:, z, 0:7, 0], wa_s.at[h])
            sent(kv0.at[0:7], kb_s.at[h])
        sent(qbuf.at[0:3], q_s)
        sent(osend.at[0:7], o_s)
        sent(ow.at[0:7], ow_s)
        sent(nbuf.at[0:3], n_s)
        sent(w.at[:, 0:7], wb_s)
        sent(w, wr_s)

    def finish():
        total = mid[...].astype(F32) + pown[x] + precv[0].astype(F32) + precv[1].astype(F32)
        out_ref[...] = total.astype(BF16)
        sent(psend.at[0:3], p_s)

    drain()
    arrived(precv, p_r.at[2])
    finish()


def local(
    queries, keys, values, query_gain, key_gain, residual_in, out_weight, norm_gain,
    gate_weight, up_weight, down_weight,
):
    vmem = pl.BlockSpec(memory_space=pltpu.VMEM)
    dma = pltpu.SemaphoreType.DMA
    tables = [jnp.asarray(t) for t in rope_tables()]
    return pl.pallas_call(
        layer_kernel,
        name="layer",
        out_shape=jax.ShapeDtypeStruct((ROWS, D), BF16),
        in_specs=[pl.BlockSpec(memory_space=pl.ANY)] * 13,
        out_specs=vmem,
        scratch_shapes=[
            pltpu.VMEM((TOK, HEAD), BF16),
            pltpu.VMEM((KTOK, HEAD), BF16),
            pltpu.VMEM((1, HEAD), F32),
            pltpu.VMEM((1, HEAD), F32),
            pltpu.VMEM((ROWS, D), BF16),
            pltpu.VMEM((1, D), F32),
            pltpu.VMEM((2, 4, HEAD), F32),
            pltpu.VMEM((2, GRID_WIDTH, HEAD), F32),
            pltpu.VMEM((TEAM, TOK, HEAD), BF16),
            pltpu.VMEM((NZ, 2, NY, KH, HEAD), BF16),
            pltpu.VMEM((NY, 2, NZ, KH, HEAD), BF16),
            pltpu.VMEM((3, NZ, NY, 2, 16, FFD), BF16),
            pltpu.VMEM((3, NZ, NY, 2, 16, FFD), BF16),
            pltpu.VMEM((8, HEAD, D), BF16),
            pltpu.VMEM((TEAM, TOK, 2 * HEAD), F32),
            pltpu.VMEM((TEAM, TOK, HEAD), F32),
            pltpu.VMEM((8, ROWS, (TEAM + 1) * HEAD), BF16),
            pltpu.VMEM((8, ROWS, (TEAM + 1) * HEAD), BF16),
            pltpu.VMEM((ROWS, 8 * HEAD), BF16),
            pltpu.VMEM((NX, ROWS, D), BF16),
            pltpu.VMEM((ROWS, D), BF16),
            pltpu.VMEM((NX, ROWS, D), BF16),
            pltpu.VMEM((NX, ROWS, D), F32),
            pltpu.VMEM((2, ROWS, D), BF16),
            pltpu.VMEM((2, 16, D), BF16),
            pltpu.VMEM((2, 16, D), BF16),
            dma((11,)), dma, dma,
            dma((2,)), dma((2,)),
            dma((2,)), dma((2, 2)),
            dma((2,)), dma((4,)),
            dma, dma((4, 3)),
            dma, dma((3,)),
            dma, dma((5,)),
            dma, dma,
            dma, dma((3,)),
            dma, dma((3,)),
        ],
        compiler_params=pltpu.CompilerParams(
            collective_id=0, has_side_effects=True, vmem_limit_bytes=56 * 1024 * 1024
        ),
    )(
        queries, keys, values, query_gain.reshape(1, -1), key_gain.reshape(1, -1), residual_in,
        out_weight, norm_gain.reshape(1, -1),
        *[a.reshape(2, 16, FFD) for a in (gate_weight, up_weight, down_weight.T)], *tables,
    )


def solution(mesh):
    finer = Mesh(mesh.devices.reshape(NZ, NY, NX, 2), ("z", "y", "x", "c"))
    sp, tp = ("z", "y"), ("x", "c")
    in_specs = (
        P(sp, tp),
        P(sp, None),
        P(sp, None),
        P(),
        P(),
        P(sp + tp, None),
        P(tp, None),
        P(),
        P(sp, tp),
        P(sp, tp),
        P(tp, sp),
    )
    return jax.shard_map(
        local, mesh=finer, in_specs=in_specs, out_specs=P(sp + tp, None), check_vma=False
    )
```

time: 84.9 us -> 77.5 us (0.913)
  Pallas kernels: 81.6 us -> 75.8 us
  local copies, waits for them, and re-layouts: 3.05 us -> 1.57 us
    pallas_call x1, Pallas kernels: 81.6 us -> 75.8 us  [local(): pl.pallas_call(layer_kernel, name='layer', out_shape=jax.ShapeDtypeStruct...]
    unnamed x2 -> x1, local copies, waits for them, and re-layouts: 3.05 us -> 1.57 us
where the time goes in v2:
time: 77.5 us; the launch traced here: 77.4 us
  Pallas kernels  75.8 us (98%)
  local copies, waits for them, and re-layouts  1.57 us (2%)
    pallas_call x1, Pallas kernels, local(): pl.pallas_call(layer_kernel, name='layer', out_shape=jax.ShapeDtypeStruct...  75.8 us
    unnamed x1, local copies, waits for them, and re-layouts  1.57 us

profile of v2, /device:TPU:1, one launch (start us, length us, event | category | flops | bytes accessed | tf_op | source)
XLA Modules:
  0.0 77.4 jit_solution(671040148502154773)
XLA Ops:
  0.0 75.8 %layer.1 = bf16[32,2048]{1,0:T(8,128)(2,1)} custom-call(bf16[256,128]{1,0:T(8,128)(2,1)} %q_hbm.1, bf16[256,256]{1,0:T(8,128)(2,1)} %k_hbm.1, bf16[256,256]{1,0:T(8,128)(2,1)} %v_hbm.1, f32[1,128]{1,0:T(1,128)} %bitcast.12, f32[1,128]{1,0:T(1,128)} %bitcast.13, bf16[32,2048]{1,0:T(8,128)(2,1)} %res_hbm.1, bf16[128,2048]{1,0:T(8,128)(2,1)} %ow_hbm.1, ...), custom_call_target="tpu_custom_call" | custom-call | tf_op jit(solution)/shard_map/layer/pallas_call | solution.py:497
  75.8 1.6 %copy.15 = bf16[32,2048]{1,0:T(8,128)(2,1)} copy(bf16[32,2048]{1,0:T(8,128)(2,1)} %layer.1) | data formatting | bytes 262144

commit v3 on v2

--- a/solution.py
+++ b/solution.py
@@ -159,30 +159,30 @@
         dev = {"y": wrap(y + d)} if h == 0 else {"z": wrap(z + d)}
         return remote(ref, ref, ka_s.at[h], ka_r.at[h], dev)
 
-    def wa(h, d, part):
-        pick = slice(0, 2) if part == 0 else slice(2, 3)
-        ref = w.at[pick, z, y, h]
-        dev = {"y": wrap(y + d)} if h == 0 else {"z": wrap(z + d)}
-        return remote(ref, ref, wa_s.at[h], wa_r.at[part, h], dev)
-
-    def w_first(part):
-        for d in FAR_FIRST:
-            wa(0, d, part).start()
-            wa(1, d, part).start()
-
-    def w_first_in(part):
-        pick = slice(0, 2) if part == 0 else slice(2, 3)
-        arrived(w.at[pick, z, 0:7, 0], wa_r.at[part, 0])
-        arrived(w.at[pick, 0:7, y, 1], wa_r.at[part, 1])
+    def wa(h, d, k):
+        shift = (k - 1) * (-1 if d == 0 else 1)
+        pick = slice(0, 3) if k < 4 else (slice(0, 2) if d == 0 else slice(2, 3))
+        ref = w.at[pick, z, wrap(y + shift), 0] if h == 0 else w.at[pick, wrap(z + shift), y, 1]
+        step = 1 if d == 0 else -1
+        dev = {"y": wrap(y + step)} if h == 0 else {"z": wrap(z + step)}
+        return remote(ref, ref, wa_s, wa_r.at[k - 1], dev)
+
+    def w_first(k):
+        if k > 1:
+            arrived(w.at[:, z, 0 : 4 if k < 5 else 2, 0], wa_r.at[k - 2])
+        if k <= 4:
+            for h in range(2):
+                for d in range(2):
+                    wa(h, d, k).start()
 
     def start_kva(d):
         kva(0, d).start()
         kva(1, d).start()
 
+    landed(w.at[:, z, y], in_s.at[10])
+    w_first(1)
     for d in FAR_FIRST:
         start_kva(d)
-    landed(w.at[:, z, y], in_s.at[10])
-    w_first(0)
 
     loads[4].wait()
     loads[5].wait()
@@ -243,16 +243,16 @@
         buf = kv0 if h == 0 else kv1
         ref = buf.at[wrap(pos[h] + shift), m]
         dev = {axis[h]: wrap(pos[h] + (1 if d == 0 else -1))}
-        return remote(ref, ref, kb_s.at[h], kb_r.at[k - 1], dev)
-
-    def kv_steps(k):
-        return [(h, d, m) for m in range(2) for h in range(2) for d in range(2) if k < 4 or d == m]
-
-    def kv_send(k):
+        return remote(ref, ref, kb_s.at[h], kb_r.at[k - 1, m], dev)
+
+    def kv_pass(k, m):
         if k > 1:
-            arrived(kv0.at[0:4], kb_r.at[k - 2])
-        for h, d, m in kv_steps(k):
-            kvb(h, d, k, m).start()
+            arrived(kv0.at[0 : 2 if k < 5 else 1], kb_r.at[k - 2, m])
+        if k <= 4:
+            for h in range(2):
+                for d in range(2):
+                    if k < 4 or d == m:
+                        kvb(h, d, k, m).start()
 
     def w_block(h, b, m, lo, hi):
         if h == 0:
@@ -309,19 +309,23 @@
             acc[h] = acc[h] * jnp.concatenate([factor, factor], axis=1) + update
             scores = later
 
+    w_first(2)
     arrived(kv0.at[0, :, 0:7], ka_r.at[0])
     arrived(kv0.at[0, :, 0:7], ka_r.at[1])
-    kv_send(1)
+    w_first(3)
+    kv_pass(1, 0)
+    kv_pass(1, 1)
     arrived(qbuf.at[0:3], q_r)
-    w_first_in(0)
+    attend([(kv0, z), (kv1, y)])
+    w_first(4)
+    kv_pass(2, 0)
+    kv_pass(2, 1)
+    attend([(kv0, wrap(z - 1)), (kv0, wrap(z + 1)), (kv1, wrap(y - 1)), (kv1, wrap(y + 1))])
+    w_first(5)
     pump(1, 0)
-    attend([(kv0, z), (kv1, y)])
-    kv_send(2)
+    kv_pass(3, 0)
+    kv_pass(3, 1)
     pump(1, 1)
-    w_first(1)
-    attend([(kv0, wrap(z - 1)), (kv0, wrap(z + 1)), (kv1, wrap(y - 1)), (kv1, wrap(y + 1))])
-    kv_send(3)
-    pump(2, 0)
     ow_in[0].wait_recv()
     ow_out[3].start()
     ow_in[1].wait_recv()
@@ -329,14 +333,15 @@
     ow_out[5].start()
     ow_out[6].start()
     attend([(kv0, wrap(z - 2)), (kv0, wrap(z + 2)), (kv1, wrap(y - 2)), (kv1, wrap(y + 2))])
-    kv_send(4)
+    kv_pass(4, 0)
+    kv_pass(4, 1)
+    pump(1, 2)
+    attend([(kv0, wrap(z - 3)), (kv0, wrap(z + 3)), (kv1, wrap(y - 3)), (kv1, wrap(y + 3))])
+    pump(2, 0)
+    kv_pass(5, 0)
+    kv_pass(5, 1)
+    attend([(kv0, wrap(z + 4)), (kv1, wrap(y + 4))])
     pump(2, 1)
-    attend([(kv0, wrap(z - 3)), (kv0, wrap(z + 3)), (kv1, wrap(y - 3)), (kv1, wrap(y + 3))])
-    w_first_in(1)
-    pump(1, 2)
-    arrived(kv0.at[0:2], kb_r.at[3])
-    attend([(kv0, wrap(z + 4)), (kv1, wrap(y + 4))])
-    pump(3, 0)
 
     lane = lax.broadcasted_iota(jnp.int32, (TOK, HEAD), 1)
     stats = jnp.zeros((TOK, HEAD), F32)
@@ -361,12 +366,12 @@
         ocopy(d).start()
     orecv[tp] = osend[tp]
 
-    pump(3, 1)
+    pump(2, 2)
     ow_in[2].wait_recv()
     ow_out[7].start()
     ow_in[3].wait_recv()
     ow_out[8].start()
-    pump(2, 2)
+    pump(3, 0)
 
     arrived(orecv.at[0:7], o_r)
     for t in range(2):
@@ -412,13 +417,15 @@
     ]
     for copy in n_out[:4]:
         copy.start()
+    pump(3, 1)
+    pump(3, 2)
     pump(4, 0)
     n_in[0].wait_recv()
     n_out[4].start()
     n_in[1].wait_recv()
     n_out[5].start()
     pump(4, 1)
-    pump(3, 2)
+    pump(4, 2)
     pump(5, 0)
     pump(5, 1)
     arrived(nbuf.at[0:2], n_r.at[2])
@@ -433,43 +440,59 @@
         return (gate_part / (1.0 + jnp.exp(-gate_part)) * lifted).astype(BF16)
 
     hidden = hidden_of(w)
-    pump(4, 2)
     all_of(0).wait_recv()
     all_of(1).wait_recv()
     hidden_p = hidden_of(wp)
     pump(5, 2)
     all_of(2).wait_recv()
-    parts = lax.dot_general(hidden, w[2].reshape(D, FFD), NT, preferred_element_type=F32)
-    parts = parts + lax.dot_general(hidden_p, wp[2].reshape(D, FFD), NT, preferred_element_type=F32)
-    parts = parts.reshape(NX, ROWS, D)
-    psend[...] = parts.astype(BF16)
-    pown[...] = parts
-
     def pcopy(n, src, dst, dev):
-        return remote(src, dst, p_s, p_r.at[min(n, 2)], dev)
-
-    p_copies = [
-        pcopy(0, psend.at[xf, low], pfar.at[0], right_x),
-        pcopy(1, psend.at[xf, high], pfar.at[1], left_x),
-        pcopy(2, psend.at[xr, high], precv.at[0, high], right_x),
-        pcopy(3, psend.at[xl, low], precv.at[1, low], left_x),
-        pcopy(4, pmix.at[0], precv.at[0, low], right_x),
-        pcopy(5, pmix.at[1], precv.at[1, high], left_x),
-    ]
-    for copy in p_copies[:4]:
-        copy.start()
-    p_copies[0].wait_recv()
-    pmix[0] = (pown[xr, low] + pfar[0].astype(F32)).astype(BF16)
-    p_copies[4].start()
-    p_copies[1].wait_recv()
-    pmix[1] = (pown[xl, high] + pfar[1].astype(F32)).astype(BF16)
-    p_copies[5].start()
+        return remote(src, dst, p_s, p_r.at[n], dev)
+
+    def parts_of(cut):
+        rows = (slice(None), slice(None), slice(None))
+        pick = (2, slice(4 * cut, 4 * cut + 4)) + rows
+        parts = lax.dot_general(hidden, w[pick].reshape(D // 2, FFD), NT, preferred_element_type=F32)
+        parts = parts + lax.dot_general(
+            hidden_p, wp[pick].reshape(D // 2, FFD), NT, preferred_element_type=F32
+        )
+        parts = parts.reshape(NX, ROWS, D // 2)
+        psend[cut] = parts.astype(BF16)
+        pown[cut] = parts
+
+    def far_copy(cut, d):
+        if d == 0:
+            return pcopy(2 * cut, psend.at[cut, xf, low], pfar.at[cut, 0], right_x)
+        return pcopy(2 * cut + 1, psend.at[cut, xf, high], pfar.at[cut, 1], left_x)
+
+    def near_copies(cut):
+        return [
+            pcopy(4, psend.at[cut, xr, high], precv.at[cut, 0, high], right_x),
+            pcopy(4, psend.at[cut, xl, low], precv.at[cut, 1, low], left_x),
+        ]
+
+    def mix(cut):
+        far_copy(cut, 0).wait_recv()
+        pmix[cut, 0] = (pown[cut, xr, low] + pfar[cut, 0].astype(F32)).astype(BF16)
+        pcopy(4, pmix.at[cut, 0], precv.at[cut, 0, low], right_x).start()
+        far_copy(cut, 1).wait_recv()
+        pmix[cut, 1] = (pown[cut, xl, high] + pfar[cut, 1].astype(F32)).astype(BF16)
+        pcopy(4, pmix.at[cut, 1], precv.at[cut, 1, high], left_x).start()
+
+    for cut in range(2):
+        parts_of(cut)
+        far_copy(cut, 0).start()
+        far_copy(cut, 1).start()
+    for cut in range(2):
+        for copy in near_copies(cut):
+            copy.start()
+    mix(0)
+    mix(1)
 
     def drain():
         for h in range(2):
             sent(kv0.at[0, :, 0:7], ka_s.at[h])
-            sent(w.at[:, z, 0:7, 0], wa_s.at[h])
             sent(kv0.at[0:7], kb_s.at[h])
+        sent(w.at[:, z, 0:7], wa_s)
         sent(qbuf.at[0:3], q_s)
         sent(osend.at[0:7], o_s)
         sent(ow.at[0:7], ow_s)
@@ -478,12 +501,15 @@
         sent(w, wr_s)
 
     def finish():
-        total = mid[...].astype(F32) + pown[x] + precv[0].astype(F32) + precv[1].astype(F32)
-        out_ref[...] = total.astype(BF16)
-        sent(psend.at[0:3], p_s)
+        for cut in range(2):
+            columns = slice(cut * D // 2, (cut + 1) * D // 2)
+            total = mid[:, columns].astype(F32) + pown[cut, x]
+            total = total + precv[cut, 0].astype(F32) + precv[cut, 1].astype(F32)
+            out_ref[:, columns] = total.astype(BF16)
+        sent(psend.at[:, 0:3], p_s)
 
     drain()
-    arrived(precv, p_r.at[2])
+    arrived(precv, p_r.at[4])
     finish()
 
 
@@ -522,21 +548,21 @@
             pltpu.VMEM((ROWS, 8 * HEAD), BF16),
             pltpu.VMEM((NX, ROWS, D), BF16),
             pltpu.VMEM((ROWS, D), BF16),
-            pltpu.VMEM((NX, ROWS, D), BF16),
-            pltpu.VMEM((NX, ROWS, D), F32),
-            pltpu.VMEM((2, ROWS, D), BF16),
-            pltpu.VMEM((2, 16, D), BF16),
-            pltpu.VMEM((2, 16, D), BF16),
+            pltpu.VMEM((2, NX, ROWS, D // 2), BF16),
+            pltpu.VMEM((2, NX, ROWS, D // 2), F32),
+            pltpu.VMEM((2, 2, ROWS, D // 2), BF16),
+            pltpu.VMEM((2, 2, 16, D // 2), BF16),
+            pltpu.VMEM((2, 2, 16, D // 2), BF16),
             dma((11,)), dma, dma,
             dma((2,)), dma((2,)),
-            dma((2,)), dma((2, 2)),
-            dma((2,)), dma((4,)),
+            dma, dma((4,)),
+            dma((2,)), dma((4, 2)),
             dma, dma((4, 3)),
             dma, dma((3,)),
             dma, dma((5,)),
             dma, dma,
             dma, dma((3,)),
-            dma, dma((3,)),
+            dma, dma((5,)),
         ],
         compiler_params=pltpu.CompilerParams(
             collective_id=0, has_side_effects=True, vmem_limit_bytes=56 * 1024 * 1024

time: 77.5 us -> 74.3 us (0.959)
  Pallas kernels: 75.8 us -> 72.6 us
    pallas_call x1, Pallas kernels: 75.8 us -> 72.6 us  [local(): pl.pallas_call(layer_kernel, name='layer', out_shape=jax.ShapeDtypeStruct...]
where the time goes in v3:
time: 74.3 us; the launch traced here: 74.2 us
  Pallas kernels  72.6 us (98%)
  local copies, waits for them, and re-layouts  1.57 us (2%)
    pallas_call x1, Pallas kernels, local(): pl.pallas_call(layer_kernel, name='layer', out_shape=jax.ShapeDtypeStruct...  72.6 us
    unnamed x1, local copies, waits for them, and re-layouts  1.57 us

profile of v3, /device:TPU:1, one launch (start us, length us, event | category | flops | bytes accessed | tf_op | source)
XLA Modules:
  0.0 74.2 jit_solution(14806916449914088609)
XLA Ops:
  0.0 72.6 %layer.1 = bf16[32,2048]{1,0:T(8,128)(2,1)} custom-call(bf16[256,128]{1,0:T(8,128)(2,1)} %q_hbm.1, bf16[256,256]{1,0:T(8,128)(2,1)} %k_hbm.1, bf16[256,256]{1,0:T(8,128)(2,1)} %v_hbm.1, f32[1,128]{1,0:T(1,128)} %bitcast.12, f32[1,128]{1,0:T(1,128)} %bitcast.13, bf16[32,2048]{1,0:T(8,128)(2,1)} %res_hbm.1, bf16[128,2048]{1,0:T(8,128)(2,1)} %ow_hbm.1, ...), custom_call_target="tpu_custom_call" | custom-call | tf_op jit(solution)/shard_map/layer/pallas_call | solution.py:523
  72.6 1.6 %copy.15 = bf16[32,2048]{1,0:T(8,128)(2,1)} copy(bf16[32,2048]{1,0:T(8,128)(2,1)} %layer.1) | data formatting | bytes 262144

commit v4 on v3

--- a/solution.py
+++ b/solution.py
@@ -28,7 +28,7 @@
 F32 = jnp.float32
 BF16 = jnp.bfloat16
 NT = (((1,), (1,)), ((), ()))
-FAR_FIRST = (4, 3, 5, 2, 6, 1, 7)
+FAR_FIRST = (4, 1, 7, 3, 5, 2, 6)
 
 
 def rope_tables():
@@ -69,7 +69,7 @@
     out_ref,
     q_ref, k_ref, qg_ref, kg_ref, res_ref, ng_ref, row_ref, col_ref,
     qbuf, kv0, kv1, w, wp, ow, acc, peak, osend, orecv, att, nbuf, mid, psend, pown, precv, pfar, pmix,
-    in_s, q_s, q_r, ka_s, ka_r, wa_s, wa_r, kb_s, kb_r, wb_s, wb_r, wr_s, wr_r,
+    in_s, q_s, q_r, ka_s, ka_r, wa_s, wa_r, wo_s, wo_r, kb_s, kb_r, wb_s, wb_r, wr_s, wr_r, wro_r,
     ow_s, ow_r, o_s, o_r, n_s, n_r, p_s, p_r,
 ):
     z = lax.axis_index("z")
@@ -116,11 +116,14 @@
         (ng_hbm, ng_ref),
         (v_hbm.at[key_rows(0), lanes], kv0.at[z, 1, y]),
         (v_hbm.at[key_rows(1), lanes], kv1.at[y, 1, z]),
-        (gate_hbm, w.at[0, z, y]),
-        (up_hbm, w.at[1, z, y]),
-        (down_hbm, w.at[2, z, y]),
+        (gate_hbm.at[0], w.at[0, 0, z, 0]),
+        (gate_hbm.at[1], w.at[1, 0, y, 0]),
+        (up_hbm.at[0], w.at[0, 1, z, 0]),
+        (up_hbm.at[1], w.at[1, 1, y, 0]),
+        (down_hbm.at[0], w.at[0, 2, z, 0]),
+        (down_hbm.at[1], w.at[1, 2, y, 0]),
     ]
-    sems = [in_s.at[n] for n in (0, 1, 2, 3, 4, 5, 6, 7, 8, 9, 9, 10, 10, 10)]
+    sems = [in_s.at[n] for n in (0, 1, 2, 3, 4, 5, 6, 7, 8, 9, 9, 10, 10, 10, 10, 10, 10)]
     loads = [pltpu.make_async_copy(a, b, m) for (a, b), m in zip(loads, sems)]
 
     def landed(ref, sem):
@@ -157,32 +160,73 @@
     def kva(h, d):
         ref = kv0.at[z, :, y] if h == 0 else kv1.at[y, :, z]
         dev = {"y": wrap(y + d)} if h == 0 else {"z": wrap(z + d)}
-        return remote(ref, ref, ka_s.at[h], ka_r.at[h], dev)
+        return remote(ref, ref, ka_s.at[h], ka_r.at[min(d, RING - d) - 1], dev)
 
     def wa(h, d, k):
-        shift = (k - 1) * (-1 if d == 0 else 1)
+        src, dst = ((1 - k) % RING, -k % RING) if d == 0 else (k - 1, k)
         pick = slice(0, 3) if k < 4 else (slice(0, 2) if d == 0 else slice(2, 3))
-        ref = w.at[pick, z, wrap(y + shift), 0] if h == 0 else w.at[pick, wrap(z + shift), y, 1]
         step = 1 if d == 0 else -1
         dev = {"y": wrap(y + step)} if h == 0 else {"z": wrap(z + step)}
-        return remote(ref, ref, wa_s, wa_r.at[k - 1], dev)
+        return remote(
+            w.at[h, pick, pos[h], src], w.at[h, pick, pos[h], dst], wa_s, wa_r.at[k - 1], dev
+        )
+
+    def four(k):
+        return w.at[0, :, 0 : 4 if k < 5 else 2, 0]
 
     def w_first(k):
         if k > 1:
-            arrived(w.at[:, z, 0 : 4 if k < 5 else 2, 0], wa_r.at[k - 2])
+            arrived(four(k), wa_r.at[k - 2])
         if k <= 4:
             for h in range(2):
                 for d in range(2):
                     wa(h, d, k).start()
 
+    def own_ref(buf, h, d, k, shift):
+        pick = slice(0, 3) if k < 4 else (slice(0, 2) if d == 0 else slice(2, 3))
+        return buf.at[h, pick, wrap(pos[h] + shift * (-1 if d == 0 else 1)), 0]
+
+    def own_pass(k):
+        if k > 1:
+            arrived(four(k), wo_r.at[k - 2])
+        for h in range(2):
+            for d in range(2):
+                if k <= 4:
+                    ref = own_ref(w, h, d, k, k - 1)
+                    dev = {axis[h]: wrap(pos[h] + (1 if d == 0 else -1))}
+                    remote(ref, ref, wo_s, wo_r.at[k - 1], dev).start()
+        for h in range(2):
+            for d in range(2):
+                if k > 1:
+                    src, dst = own_ref(w, h, d, k - 1, k - 1), own_ref(wp, h, d, k - 1, k - 1)
+                    remote(src, dst, wr_s, wro_r, partner).start()
+                elif d == 0:
+                    src, dst = own_ref(w, h, d, 1, 0), own_ref(wp, h, d, 1, 0)
+                    remote(src, dst, wr_s, wro_r, partner).start()
+
+    def kv_piece(h, e):
+        ref = kv0.at[z, :, wrap(y + e)] if h == 0 else kv1.at[y, :, wrap(z + e)]
+        for d in range(2):
+            dev = {axis[h]: wrap(pos[h] + (1 if d == 0 else -1))}
+            remote(ref, ref, kb_s.at[h], kb_r.at[0, 0], dev).start()
+
+    def kv_group(g):
+        if g > 0:
+            arrived(kv0.at[0, :, 0 : 4 if g < 4 else 2], ka_r.at[g - 1])
+        for h in range(2):
+            for e in sorted({g % RING, -g % RING}):
+                kv_piece(h, e)
+
     def start_kva(d):
         kva(0, d).start()
         kva(1, d).start()
 
-    landed(w.at[:, z, y], in_s.at[10])
+    kv_group(0)
+    landed(w.at[:, :, 0, 0], in_s.at[10])
     w_first(1)
     for d in FAR_FIRST:
         start_kva(d)
+    own_pass(1)
 
     loads[4].wait()
     loads[5].wait()
@@ -238,53 +282,46 @@
     for n in range(3):
         ow_out[n].start()
 
-    def kvb(h, d, k, m):
+    def kvb(h, d, k, q):
         shift = (k - 1) * (-1 if d == 0 else 1)
         buf = kv0 if h == 0 else kv1
-        ref = buf.at[wrap(pos[h] + shift), m]
+        ref = buf.at[wrap(pos[h] + shift), q // 2, pl.ds(4 * (q % 2), 4)]
         dev = {axis[h]: wrap(pos[h] + (1 if d == 0 else -1))}
-        return remote(ref, ref, kb_s.at[h], kb_r.at[k - 1, m], dev)
-
-    def kv_pass(k, m):
-        if k > 1:
-            arrived(kv0.at[0 : 2 if k < 5 else 1], kb_r.at[k - 2, m])
-        if k <= 4:
-            for h in range(2):
-                for d in range(2):
-                    if k < 4 or d == m:
-                        kvb(h, d, k, m).start()
-
-    def w_block(h, b, m, lo, hi):
-        if h == 0:
-            return lambda buf: buf.at[m, b, lo:hi, 0]
-        return lambda buf: buf.at[m, lo:hi, b, 1]
-
-    def wb(h, d, k, m):
-        shift = (k - 1) * (-1 if d == 0 else 1)
-        lo, hi = (0, RING) if k < 4 else ((0, 4) if d == 0 else (4, RING))
-        ref = w_block(h, wrap(pos[h] + shift), m, lo, hi)(w)
-        dev = {axis[h]: wrap(pos[h] + (1 if d == 0 else -1))}
-        return remote(ref, ref, wb_s, wb_r.at[k - 1, m], dev)
-
-    def hand_over(h, d, k, m):
-        shift = k * (-1 if d == 0 else 1)
-        lo, hi = (0, RING) if k < 4 else ((0, 4) if d == 0 else (4, RING))
-        pick = w_block(h, wrap(pos[h] + shift), m, lo, hi)
-        remote(pick(w), pick(wp), wr_s, wr_r.at[m], partner).start()
+        return remote(ref, ref, kb_s.at[h], kb_r.at[k - 1, q], dev)
+
+    def kv_pass(k):
+        if k == 2:
+            arrived(kv0.at[0:4], kb_r.at[0, 0])
+        for q in range(4):
+            if k > 2:
+                arrived(kv0.at[0, 0 : 2 if k < 5 else 1], kb_r.at[k - 2, q])
+            if k <= 4:
+                for h in range(2):
+                    for d in range(2):
+                        if k < 4 or d == q // 2:
+                            kvb(h, d, k, q).start()
+
+    def rest(buf, h, d, k, m, shift):
+        lo, hi = (1, RING) if k < 4 else ((1, 5) if d == 0 else (5, RING))
+        return buf.at[h, m, wrap(pos[h] + shift * (-1 if d == 0 else 1)), lo:hi]
 
     def pump(k, m):
         if k > 1:
-            arrived(w.at[m, 0 : 2 if k < 5 else 1], wb_r.at[k - 2, m])
-        if k <= 4:
-            for h in range(2):
-                for d in range(2):
-                    wb(h, d, k, m).start()
+            arrived(w.at[0, m, 0 : 4 if k < 5 else 2, 1:RING], wb_r.at[k - 2, m])
+        for h in range(2):
+            for d in range(2):
+                if k <= 4:
+                    ref = rest(w, h, d, k, m, k - 1)
+                    dev = {axis[h]: wrap(pos[h] + (1 if d == 0 else -1))}
+                    remote(ref, ref, wb_s, wb_r.at[k - 1, m], dev).start()
         for h in range(2):
             for d in range(2):
                 if k > 1:
-                    hand_over(h, d, k - 1, m)
+                    src, dst = rest(w, h, d, k - 1, m, k - 1), rest(wp, h, d, k - 1, m, k - 1)
+                    remote(src, dst, wr_s, wr_r.at[m], partner).start()
                 elif d == 0:
-                    hand_over(h, 0, 0, m)
+                    src, dst = rest(w, h, d, 1, m, 0), rest(wp, h, d, 1, m, 0)
+                    remote(src, dst, wr_s, wr_r.at[m], partner).start()
 
     ones = jnp.ones((1, HEAD), BF16)
 
@@ -310,22 +347,22 @@
             scores = later
 
     w_first(2)
-    arrived(kv0.at[0, :, 0:7], ka_r.at[0])
-    arrived(kv0.at[0, :, 0:7], ka_r.at[1])
+    kv_group(1)
+    kv_group(2)
+    kv_group(3)
+    kv_group(4)
     w_first(3)
-    kv_pass(1, 0)
-    kv_pass(1, 1)
+    own_pass(2)
     arrived(qbuf.at[0:3], q_r)
     attend([(kv0, z), (kv1, y)])
+    kv_pass(2)
     w_first(4)
-    kv_pass(2, 0)
-    kv_pass(2, 1)
+    own_pass(3)
     attend([(kv0, wrap(z - 1)), (kv0, wrap(z + 1)), (kv1, wrap(y - 1)), (kv1, wrap(y + 1))])
+    kv_pass(3)
     w_first(5)
+    own_pass(4)
     pump(1, 0)
-    kv_pass(3, 0)
-    kv_pass(3, 1)
-    pump(1, 1)
     ow_in[0].wait_recv()
     ow_out[3].start()
     ow_in[1].wait_recv()
@@ -333,29 +370,30 @@
     ow_out[5].start()
     ow_out[6].start()
     attend([(kv0, wrap(z - 2)), (kv0, wrap(z + 2)), (kv1, wrap(y - 2)), (kv1, wrap(y + 2))])
-    kv_pass(4, 0)
-    kv_pass(4, 1)
+    kv_pass(4)
+    pump(1, 1)
     pump(1, 2)
     attend([(kv0, wrap(z - 3)), (kv0, wrap(z + 3)), (kv1, wrap(y - 3)), (kv1, wrap(y + 3))])
+    own_pass(5)
+    kv_pass(5)
+    attend([(kv0, wrap(z + 4)), (kv1, wrap(y + 4))])
     pump(2, 0)
-    kv_pass(5, 0)
-    kv_pass(5, 1)
-    attend([(kv0, wrap(z + 4)), (kv1, wrap(y + 4))])
     pump(2, 1)
 
     lane = lax.broadcasted_iota(jnp.int32, (TOK, HEAD), 1)
-    stats = jnp.zeros((TOK, HEAD), F32)
+    tops = jnp.zeros((TOK, HEAD), F32)
+    sums = jnp.ones((TOK, HEAD), F32)
     for h in range(TEAM):
         total = acc[h, :, HEAD:]
         mean = (acc[h, :, :HEAD] / total).astype(BF16)
         osend[:, :, h * HEAD : (h + 1) * HEAD] = mean.reshape(8, ROWS, HEAD)
-        level = peak[h] + jnp.log2(total)
-        first = level.astype(BF16).astype(F32)
-        second = (level - first).astype(BF16).astype(F32)
-        third = level - first - second
-        stats = jnp.where(lane == h, first, stats)
-        stats = jnp.where(lane == h + 4, second, stats)
-        stats = jnp.where(lane == h + 8, third, stats)
+        tops = jnp.where(lane == h, peak[h], tops)
+        sums = jnp.where(lane == h, total, sums)
+    level = tops + jnp.log2(sums)
+    first = level.astype(BF16).astype(F32)
+    second = (level - first).astype(BF16).astype(F32)
+    third = level - first - second
+    stats = first + pltpu.roll(second, 4, 1) + pltpu.roll(third, 8, 1)
     osend[:, :, TEAM * HEAD :] = stats.astype(BF16).reshape(8, ROWS, HEAD)
 
     def ocopy(d):
@@ -375,20 +413,21 @@
 
     arrived(orecv.at[0:7], o_r)
     for t in range(2):
+        levels = []
+        for i in range(t * TEAM, (t + 1) * TEAM):
+            st = orecv[i, :, TEAM * HEAD :].astype(F32)
+            levels.append(st + pltpu.roll(st, HEAD - 4, 1) + pltpu.roll(st, HEAD - 8, 1))
+        top = jnp.maximum(jnp.maximum(levels[0], levels[1]), jnp.maximum(levels[2], levels[3]))
+        shares = [jnp.exp2(v - top) for v in levels]
+        total = shares[0] + shares[1] + shares[2] + shares[3]
+        shares = [v / total for v in shares]
         for h in range(TEAM):
-            levels = []
-            for i in range(t * TEAM, (t + 1) * TEAM):
-                st = orecv[i, :, TEAM * HEAD :].astype(F32)
-                levels.append(st[:, h : h + 1] + st[:, h + 4 : h + 5] + st[:, h + 8 : h + 9])
-            top = jnp.maximum(jnp.maximum(levels[0], levels[1]), jnp.maximum(levels[2], levels[3]))
-            shares = [jnp.exp2(v - top) for v in levels]
-            total = shares[0] + shares[1] + shares[2] + shares[3]
             mixed = jnp.zeros((ROWS, HEAD), F32)
             for i in range(TEAM):
                 block = orecv[t * TEAM + i, :, h * HEAD : (h + 1) * HEAD].astype(F32)
-                mixed = mixed + block * shares[i]
+                mixed = mixed + block * shares[i][:, h : h + 1]
             at = (t * TEAM + h) * HEAD
-            att[:, at : at + HEAD] = (mixed / total).astype(BF16)
+            att[:, at : at + HEAD] = mixed.astype(BF16)
 
     arrived(ow.at[0:4], ow_r.at[4])
     loads[7].wait()
@@ -432,32 +471,36 @@
     normed = nbuf[...].reshape(NX * ROWS, D)
 
     def all_of(m):
-        return remote(w.at[m], wp.at[m], wr_s, wr_r.at[m], partner)
+        return remote(w.at[:, m, :, 1:RING], wp.at[:, m, :, 1:RING], wr_s, wr_r.at[m], partner)
+
+    back_y = [wrap(i - y) for i in range(RING)]
+    back_z = [wrap(i - z) for i in range(RING)]
+
+    def matrix(buf, m, places=range(NZ)):
+        blocks = []
+        for i in places:
+            for k in range(NY):
+                blocks += [buf[0, m, i, back_y[k]], buf[1, m, k, back_z[i]]]
+        return jnp.concatenate(blocks, axis=0)
 
     def hidden_of(buf):
-        gate_part = jnp.dot(normed, buf[0].reshape(D, FFD), preferred_element_type=F32)
-        lifted = jnp.dot(normed, buf[1].reshape(D, FFD), preferred_element_type=F32)
+        gate_part = jnp.dot(normed, matrix(buf, 0), preferred_element_type=F32)
+        lifted = jnp.dot(normed, matrix(buf, 1), preferred_element_type=F32)
         return (gate_part / (1.0 + jnp.exp(-gate_part)) * lifted).astype(BF16)
 
     hidden = hidden_of(w)
+    arrived(w.at[:, :, :, 0], wro_r)
     all_of(0).wait_recv()
     all_of(1).wait_recv()
     hidden_p = hidden_of(wp)
     pump(5, 2)
-    all_of(2).wait_recv()
     def pcopy(n, src, dst, dev):
         return remote(src, dst, p_s, p_r.at[n], dev)
 
-    def parts_of(cut):
-        rows = (slice(None), slice(None), slice(None))
-        pick = (2, slice(4 * cut, 4 * cut + 4)) + rows
-        parts = lax.dot_general(hidden, w[pick].reshape(D // 2, FFD), NT, preferred_element_type=F32)
-        parts = parts + lax.dot_general(
-            hidden_p, wp[pick].reshape(D // 2, FFD), NT, preferred_element_type=F32
-        )
-        parts = parts.reshape(NX, ROWS, D // 2)
-        psend[cut] = parts.astype(BF16)
-        pown[cut] = parts
+    def parts_of(left, buf, cut):
+        places = range(4 * cut, 4 * cut + 4)
+        parts = lax.dot_general(left, matrix(buf, 2, places), NT, preferred_element_type=F32)
+        return parts.reshape(NX, ROWS, D // 2)
 
     def far_copy(cut, d):
         if d == 0:
@@ -479,7 +522,12 @@
         pcopy(4, pmix.at[cut, 1], precv.at[cut, 1, high], left_x).start()
 
     for cut in range(2):
-        parts_of(cut)
+        pown[cut] = parts_of(hidden, w, cut)
+    all_of(2).wait_recv()
+    for cut in range(2):
+        parts = pown[cut] + parts_of(hidden_p, wp, cut)
+        pown[cut] = parts
+        psend[cut] = parts.astype(BF16)
         far_copy(cut, 0).start()
         far_copy(cut, 1).start()
     for cut in range(2):
@@ -492,12 +540,13 @@
         for h in range(2):
             sent(kv0.at[0, :, 0:7], ka_s.at[h])
             sent(kv0.at[0:7], kb_s.at[h])
-        sent(w.at[:, z, 0:7], wa_s)
+        sent(w.at[:, :, 0:7, 0], wa_s)
+        sent(w.at[:, :, 0:7, 0], wo_s)
         sent(qbuf.at[0:3], q_s)
         sent(osend.at[0:7], o_s)
         sent(ow.at[0:7], ow_s)
         sent(nbuf.at[0:3], n_s)
-        sent(w.at[:, 0:7], wb_s)
+        sent(w.at[:, :, 0:7, 1:RING], wb_s)
         sent(w, wr_s)
 
     def finish():
@@ -538,8 +587,8 @@
             pltpu.VMEM((TEAM, TOK, HEAD), BF16),
             pltpu.VMEM((NZ, 2, NY, KH, HEAD), BF16),
             pltpu.VMEM((NY, 2, NZ, KH, HEAD), BF16),
-            pltpu.VMEM((3, NZ, NY, 2, 16, FFD), BF16),
-            pltpu.VMEM((3, NZ, NY, 2, 16, FFD), BF16),
+            pltpu.VMEM((2, 3, RING, RING, 16, FFD), BF16),
+            pltpu.VMEM((2, 3, RING, RING, 16, FFD), BF16),
             pltpu.VMEM((8, HEAD, D), BF16),
             pltpu.VMEM((TEAM, TOK, 2 * HEAD), F32),
             pltpu.VMEM((TEAM, TOK, HEAD), F32),
@@ -554,11 +603,12 @@
             pltpu.VMEM((2, 2, 16, D // 2), BF16),
             pltpu.VMEM((2, 2, 16, D // 2), BF16),
             dma((11,)), dma, dma,
-            dma((2,)), dma((2,)),
+            dma((2,)), dma((4,)),
             dma, dma((4,)),
-            dma((2,)), dma((4, 2)),
+            dma, dma((4,)),
+            dma((2,)), dma((4, 4)),
             dma, dma((4, 3)),
-            dma, dma((3,)),
+            dma, dma((3,)), dma,
             dma, dma((5,)),
             dma, dma,
             dma, dma((3,)),

time: 74.3 us -> 70.6 us (0.950)
  Pallas kernels: 72.6 us -> 68.9 us
    pallas_call x1, Pallas kernels: 72.6 us -> 68.9 us  [local(): pl.pallas_call(layer_kernel, name='layer', out_shape=jax.ShapeDtypeStruct...]
where the time goes in v4:
time: 70.6 us; the launch traced here: 70.4 us
  Pallas kernels  68.9 us (98%)
  local copies, waits for them, and re-layouts  1.57 us (2%)
    pallas_call x1, Pallas kernels, local(): pl.pallas_call(layer_kernel, name='layer', out_shape=jax.ShapeDtypeStruct...  68.9 us
    unnamed x1, local copies, waits for them, and re-layouts  1.57 us

profile of v4, /device:TPU:1, one launch (start us, length us, event | category | flops | bytes accessed | tf_op | source)
XLA Modules:
  0.0 70.4 jit_solution(7254696322106993757)
XLA Ops:
  0.0 68.9 %layer.1 = bf16[32,2048]{1,0:T(8,128)(2,1)} custom-call(bf16[256,128]{1,0:T(8,128)(2,1)} %q_hbm.1, bf16[256,256]{1,0:T(8,128)(2,1)} %k_hbm.1, bf16[256,256]{1,0:T(8,128)(2,1)} %v_hbm.1, f32[1,128]{1,0:T(1,128)} %bitcast.12, f32[1,128]{1,0:T(1,128)} %bitcast.13, bf16[32,2048]{1,0:T(8,128)(2,1)} %res_hbm.1, bf16[128,2048]{1,0:T(8,128)(2,1)} %ow_hbm.1, ...), custom_call_target="tpu_custom_call" | custom-call | tf_op jit(solution)/shard_map/layer/pallas_call | solution.py:572
  68.9 1.6 %copy.15 = bf16[32,2048]{1,0:T(8,128)(2,1)} copy(bf16[32,2048]{1,0:T(8,128)(2,1)} %layer.1) | data formatting | bytes 262144

commit v5 on v4

--- a/solution.py
+++ b/solution.py
@@ -305,13 +305,21 @@
         lo, hi = (1, RING) if k < 4 else ((1, 5) if d == 0 else (5, RING))
         return buf.at[h, m, wrap(pos[h] + shift * (-1 if d == 0 else 1)), lo:hi]
 
+    def pump_near(m):
+        for h in range(2):
+            for d in range(2):
+                dev = {axis[h]: wrap(pos[h] + (1 if d == 0 else -1))}
+                for lo in (1, 6):
+                    ref = w.at[h, m, pos[h], lo : lo + 2]
+                    remote(ref, ref, wb_s, wb_r.at[0, m], dev).start()
+
     def pump(k, m):
         if k > 1:
             arrived(w.at[0, m, 0 : 4 if k < 5 else 2, 1:RING], wb_r.at[k - 2, m])
         for h in range(2):
             for d in range(2):
                 if k <= 4:
-                    ref = rest(w, h, d, k, m, k - 1)
+                    ref = rest(w, h, d, k, m, k - 1) if k > 1 else w.at[h, m, pos[h], 3:6]
                     dev = {axis[h]: wrap(pos[h] + (1 if d == 0 else -1))}
                     remote(ref, ref, wb_s, wb_r.at[k - 1, m], dev).start()
         for h in range(2):
@@ -357,12 +365,14 @@
     attend([(kv0, z), (kv1, y)])
     kv_pass(2)
     w_first(4)
+    pump_near(0)
     own_pass(3)
     attend([(kv0, wrap(z - 1)), (kv0, wrap(z + 1)), (kv1, wrap(y - 1)), (kv1, wrap(y + 1))])
     kv_pass(3)
+    pump_near(1)
     w_first(5)
-    own_pass(4)
     pump(1, 0)
+    pump(1, 1)
     ow_in[0].wait_recv()
     ow_out[3].start()
     ow_in[1].wait_recv()
@@ -371,14 +381,15 @@
     ow_out[6].start()
     attend([(kv0, wrap(z - 2)), (kv0, wrap(z + 2)), (kv1, wrap(y - 2)), (kv1, wrap(y + 2))])
     kv_pass(4)
-    pump(1, 1)
+    own_pass(4)
+    pump_near(2)
     pump(1, 2)
     attend([(kv0, wrap(z - 3)), (kv0, wrap(z + 3)), (kv1, wrap(y - 3)), (kv1, wrap(y + 3))])
+    pump(2, 0)
+    kv_pass(5)
+    pump(2, 1)
+    attend([(kv0, wrap(z + 4)), (kv1, wrap(y + 4))])
     own_pass(5)
-    kv_pass(5)
-    attend([(kv0, wrap(z + 4)), (kv1, wrap(y + 4))])
-    pump(2, 0)
-    pump(2, 1)
 
     lane = lax.broadcasted_iota(jnp.int32, (TOK, HEAD), 1)
     tops = jnp.zeros((TOK, HEAD), F32)
@@ -410,6 +421,7 @@
     ow_in[3].wait_recv()
     ow_out[8].start()
     pump(3, 0)
+    pump(3, 1)
 
     arrived(orecv.at[0:7], o_r)
     for t in range(2):
@@ -437,37 +449,42 @@
     mid[...] = middle
     nbuf[x] = normalize(middle.astype(F32), ng_ref[...]).astype(BF16)
 
-    def ncopy(n, ref, dev):
-        return remote(ref, ref, n_s, n_r.at[min(n, 2)], dev)
-
     xl, xr, xf = wrap(x - 1, NX), wrap(x + 1, NX), wrap(x + 2, NX)
     low, high = pl.ds(0, 16), pl.ds(16, 16)
-    n_out = [
-        ncopy(0, nbuf.at[x, low], right_x),
-        ncopy(1, nbuf.at[x, high], left_x),
-        ncopy(2, nbuf.at[x, high], right_x),
-        ncopy(3, nbuf.at[x, low], left_x),
-        ncopy(4, nbuf.at[xl, low], right_x),
-        ncopy(5, nbuf.at[xr, high], left_x),
-    ]
-    n_in = [
-        ncopy(0, nbuf.at[xl, low], right_x),
-        ncopy(1, nbuf.at[xr, high], left_x),
-    ]
-    for copy in n_out[:4]:
-        copy.start()
-    pump(3, 1)
+    halves = (pl.ds(0, D // 2), pl.ds(D // 2, D // 2))
+
+    def ncopy(n, ref, dev):
+        return remote(ref, ref, n_s, n_r.at[n], dev)
+
+    def n_far(d, p):
+        if d == 0:
+            return ncopy(p, nbuf.at[x, low, halves[p]], right_x)
+        return ncopy(2 + p, nbuf.at[x, high, halves[p]], left_x)
+
+    def n_far_on(d, p):
+        if d == 0:
+            ncopy(p, nbuf.at[xl, low, halves[p]], right_x).wait_recv()
+            ncopy(4, nbuf.at[xl, low, halves[p]], right_x).start()
+        else:
+            ncopy(2 + p, nbuf.at[xr, high, halves[p]], left_x).wait_recv()
+            ncopy(4, nbuf.at[xr, high, halves[p]], left_x).start()
+
+    for p in range(2):
+        n_far(0, p).start()
+        n_far(1, p).start()
+    ncopy(4, nbuf.at[x, high], right_x).start()
+    ncopy(4, nbuf.at[x, low], left_x).start()
     pump(3, 2)
     pump(4, 0)
-    n_in[0].wait_recv()
-    n_out[4].start()
-    n_in[1].wait_recv()
-    n_out[5].start()
+    n_far_on(0, 0)
+    n_far_on(1, 0)
     pump(4, 1)
+    n_far_on(0, 1)
+    n_far_on(1, 1)
     pump(4, 2)
     pump(5, 0)
     pump(5, 1)
-    arrived(nbuf.at[0:2], n_r.at[2])
+    arrived(nbuf.at[0:2], n_r.at[4])
     normed = nbuf[...].reshape(NX * ROWS, D)
 
     def all_of(m):
@@ -611,7 +628,7 @@
             dma, dma((3,)), dma,
             dma, dma((5,)),
             dma, dma,
-            dma, dma((3,)),
+            dma, dma((5,)),
             dma, dma((5,)),
         ],
         compiler_params=pltpu.CompilerParams(

time: 70.6 us -> 70.3 us (level)
  no operation moved by 1% of the time
where the time goes in v5:
time: 70.3 us; the launch traced here: 70.1 us
  Pallas kernels  68.5 us (97%)
  local copies, waits for them, and re-layouts  1.57 us (2%)
    pallas_call x1, Pallas kernels, local(): pl.pallas_call(layer_kernel, name='layer', out_shape=jax.ShapeDtypeStruct...  68.5 us
    unnamed x1, local copies, waits for them, and re-layouts  1.57 us

profile of v5, /device:TPU:1, one launch (start us, length us, event | category | flops | bytes accessed | tf_op | source)
XLA Modules:
  0.0 70.1 jit_solution(15958140223122523776)
XLA Ops:
  0.0 68.5 %layer.1 = bf16[32,2048]{1,0:T(8,128)(2,1)} custom-call(bf16[256,128]{1,0:T(8,128)(2,1)} %q_hbm.1, bf16[256,256]{1,0:T(8,128)(2,1)} %k_hbm.1, bf16[256,256]{1,0:T(8,128)(2,1)} %v_hbm.1, f32[1,128]{1,0:T(1,128)} %bitcast.12, f32[1,128]{1,0:T(1,128)} %bitcast.13, bf16[32,2048]{1,0:T(8,128)(2,1)} %res_hbm.1, bf16[128,2048]{1,0:T(8,128)(2,1)} %ow_hbm.1, ...), custom_call_target="tpu_custom_call" | custom-call | tf_op jit(solution)/shard_map/layer/pallas_call | solution.py:589
  68.5 1.6 %copy.15 = bf16[32,2048]{1,0:T(8,128)(2,1)} copy(bf16[32,2048]{1,0:T(8,128)(2,1)} %layer.1) | data formatting | bytes 262144

commit v6 on v5

--- a/solution.py
+++ b/solution.py
@@ -28,7 +28,7 @@
 F32 = jnp.float32
 BF16 = jnp.bfloat16
 NT = (((1,), (1,)), ((), ()))
-FAR_FIRST = (4, 1, 7, 3, 5, 2, 6)
+FAR_FIRST = (1, 7, 2, 6, 4, 3, 5)
 
 
 def rope_tables():
@@ -505,12 +505,6 @@
         lifted = jnp.dot(normed, matrix(buf, 1), preferred_element_type=F32)
         return (gate_part / (1.0 + jnp.exp(-gate_part)) * lifted).astype(BF16)
 
-    hidden = hidden_of(w)
-    arrived(w.at[:, :, :, 0], wro_r)
-    all_of(0).wait_recv()
-    all_of(1).wait_recv()
-    hidden_p = hidden_of(wp)
-    pump(5, 2)
     def pcopy(n, src, dst, dev):
         return remote(src, dst, p_s, p_r.at[n], dev)
 
@@ -538,8 +532,14 @@
         pmix[cut, 1] = (pown[cut, xl, high] + pfar[cut, 1].astype(F32)).astype(BF16)
         pcopy(4, pmix.at[cut, 1], precv.at[cut, 1, high], left_x).start()
 
+    hidden = hidden_of(w)
+    pump(5, 2)
     for cut in range(2):
         pown[cut] = parts_of(hidden, w, cut)
+    arrived(w.at[:, :, :, 0], wro_r)
+    all_of(0).wait_recv()
+    all_of(1).wait_recv()
+    hidden_p = hidden_of(wp)
     all_of(2).wait_recv()
     for cut in range(2):
         parts = pown[cut] + parts_of(hidden_p, wp, cut)

time: 70.3 us -> 69.5 us (0.989)
  no operation moved by 1% of the time
where the time goes in v6:
time: 69.5 us; the launch traced here: 69.4 us
  Pallas kernels  67.8 us (98%)
  local copies, waits for them, and re-layouts  1.57 us (2%)
    pallas_call x1, Pallas kernels, local(): pl.pallas_call(layer_kernel, name='layer', out_shape=jax.ShapeDtypeStruct...  67.8 us
    unnamed x1, local copies, waits for them, and re-layouts  1.57 us

profile of v6, /device:TPU:1, one launch (start us, length us, event | category | flops | bytes accessed | tf_op | source)
XLA Modules:
  0.0 69.4 jit_solution(1602189515480209334)
XLA Ops:
  0.0 67.8 %layer.1 = bf16[32,2048]{1,0:T(8,128)(2,1)} custom-call(bf16[256,128]{1,0:T(8,128)(2,1)} %q_hbm.1, bf16[256,256]{1,0:T(8,128)(2,1)} %k_hbm.1, bf16[256,256]{1,0:T(8,128)(2,1)} %v_hbm.1, f32[1,128]{1,0:T(1,128)} %bitcast.12, f32[1,128]{1,0:T(1,128)} %bitcast.13, bf16[32,2048]{1,0:T(8,128)(2,1)} %res_hbm.1, bf16[128,2048]{1,0:T(8,128)(2,1)} %ow_hbm.1, ...), custom_call_target="tpu_custom_call" | custom-call | tf_op jit(solution)/shard_map/layer/pallas_call | solution.py:589
  67.8 1.6 %copy.15 = bf16[32,2048]{1,0:T(8,128)(2,1)} copy(bf16[32,2048]{1,0:T(8,128)(2,1)} %layer.1) | data formatting | bytes 262144
